TPU v7x, 256 devices: a whole 4x4x8 slice. The times are simulated.
256 devices in a mesh: rep: 2 (over z_hi), fs: 16 (over z_lo, y), tp: 8 (over x, core).
Axes of the slice: x: 4, y: 4, z: 8 (z_hi: 2, z_lo: 4; z = z_hi * 4 + z_lo), core: 2. Of those that a mesh axis runs over, the one named last changes fastest.
Arguments:
- inputs: bfloat16 [16384, 2048], P(('rep', 'fs')), may hold values from -6 to 6
- cotangent: bfloat16 [16384, 2048], P(('rep', 'fs')), may hold values from -6 to 6
- gate_pre: bfloat16 [16384, 5632], P(('rep', 'fs'), 'tp'), may hold values from -8 to 8
- up_pre: bfloat16 [16384, 5632], P(('rep', 'fs'), 'tp'), may hold values from -6 to 6
- gate_weight: float32 [2048, 5632], P('fs', 'tp'), may hold values from -0.125 to 0.125
- up_weight: float32 [2048, 5632], P('fs', 'tp'), may hold values from -0.125 to 0.125
- down_weight: float32 [2048, 5632], P('fs', 'tp'), may hold values from -0.078125 to 0.078125
- gate_scale: float32 [1, 5632], P(None, 'tp'), may hold values from 0.1 to 1.9
- up_scale: float32 [1, 5632], P(None, 'tp'), may hold values from 0.1 to 1.9
- down_scale: float32 [1, 5632], P(None, 'tp'), may hold values from 0.1 to 1.9
Outputs:
- input_grad: bfloat16 [16384, 2048], P(('rep', 'fs'), 'tp')
- gate_grad: float32 [2048, 5632], P('fs', 'tp')
- up_grad: float32 [2048, 5632], P('fs', 'tp')
- down_grad: float32 [2048, 5632], P('fs', 'tp')
All inputs are finite; a program needn't handle non-finite values.
Results may differ from a plain program's by a relative error of at most 0.018.
Values may be sent and summed in bfloat16 or wider, within the bound.
A program may use at most 128 MiB of HBM per device.

v0:
```python
import jax
import jax.numpy as jnp
from jax import lax
from jax.sharding import Mesh
from jax.sharding import PartitionSpec as P

FS = ("fs_0", "fs_1")
REP_FS = ("rep", "fs_0", "fs_1")


def in_order(parts, dim):
    lengths = list(parts.shape[1:])
    lengths[dim] *= parts.shape[0]
    return jnp.moveaxis(parts, 0, dim).reshape(lengths)


def stacked_from(value, axes, order):
    parts = value
    for k in order:
        parts = lax.all_gather(parts, axes[k])
    done = order[::-1]
    back = [done.index(k) for k in range(len(axes))]
    parts = parts.transpose(*back, *range(len(axes), parts.ndim))
    return parts.reshape(-1, *value.shape)


def whole_of(value, axes, order, dim):
    return in_order(stacked_from(value, axes, order), dim)


def split_up(value, dim, length):
    lengths = value.shape
    parts = value.reshape(*lengths[:dim], length, lengths[dim] // length, *lengths[dim + 1 :])
    return jnp.moveaxis(parts, dim, 0)


def summed_on_arrival(value, axis, dim):
    parts = split_up(value, dim, lax.axis_size(axis))
    arrived = lax.all_to_all(parts, axis, split_axis=0, concat_axis=0, tiled=True)
    return arrived.astype(jnp.float32).sum(axis=0)


def copy_for_each(value, axis):
    copies = jnp.broadcast_to(value, (lax.axis_size(axis), *value.shape))
    return lax.all_to_all(copies, axis, split_axis=0, concat_axis=0, tiled=True)


def over_copies(value, axis):
    everything = copy_for_each(value, axis)
    return jnp.sum(everything.astype(jnp.float32), axis=0)


def local(
    inputs,
    cotangent,
    gate_pre,
    up_pre,
    gate_weight,
    up_weight,
    down_weight,
    gate_scale,
    up_scale,
    down_scale,
):
    hidden_cols = gate_pre.shape[1]
    gate = gate_pre.astype(jnp.float32)
    upper = up_pre.astype(jnp.float32)
    sig = jax.nn.sigmoid(gate)
    act = gate * sig
    hidden = (act * upper).astype(jnp.bfloat16)
    hidden_cot = jnp.dot(
        cotangent,
        whole_of(down_weight.astype(jnp.bfloat16), FS, (0, 1), 0),
        preferred_element_type=jnp.float32,
    )
    hidden_cot = hidden_cot * down_scale
    gate_cot = (hidden_cot * upper * sig * (1.0 + gate * (1.0 - sig)) * gate_scale).astype(
        jnp.bfloat16
    )
    up_cot = (hidden_cot * act * up_scale).astype(jnp.bfloat16)
    both_cot = jnp.concatenate([gate_cot, up_cot], axis=1)
    both_rows = jnp.concatenate(
        [gate_weight.astype(jnp.bfloat16), up_weight.astype(jnp.bfloat16)], axis=1
    )
    partial_value = lax.dot_general(
        both_cot,
        whole_of(both_rows, FS, (0, 1), 0),
        (((1,), (1,)), ((), ())),
        preferred_element_type=jnp.float32,
    )
    input_grad = summed_on_arrival(partial_value.astype(jnp.bfloat16), "tp", 1).astype(jnp.bfloat16)
    dims = (((0,), (0,)), ((), ()))
    g_part = lax.dot_general(inputs, gate_cot, dims, preferred_element_type=jnp.float32)
    u_part = lax.dot_general(inputs, up_cot, dims, preferred_element_type=jnp.float32)
    d_part = (
        lax.dot_general(cotangent, hidden, dims, preferred_element_type=jnp.float32) * down_scale
    )
    summed = lax.psum_scatter(
        jnp.concatenate([g_part, u_part, d_part], axis=1).astype(jnp.bfloat16),
        FS,
        scatter_dimension=0,
        tiled=True,
    ).astype(jnp.float32)
    summed = over_copies(summed.astype(jnp.bfloat16), "rep").astype(jnp.float32)
    gate_grad = summed[:, :hidden_cols]
    up_grad = summed[:, hidden_cols : 2 * hidden_cols]
    down_grad = summed[:, 2 * hidden_cols :]
    return (input_grad, gate_grad, up_grad, down_grad)


def solution(mesh):
    finer = Mesh(
        mesh.devices.reshape(mesh.shape["rep"], 4, 4, mesh.shape["tp"]),
        ("rep", "fs_0", "fs_1", "tp"),
    )
    in_specs = (
        P(REP_FS, None),
        P(REP_FS, None),
        P(REP_FS, "tp"),
        P(REP_FS, "tp"),
        P(FS, "tp"),
        P(FS, "tp"),
        P(FS, "tp"),
        P(None, "tp"),
        P(None, "tp"),
        P(None, "tp"),
    )
    out_specs = (P(REP_FS, "tp"), P(FS, "tp"), P(FS, "tp"), P(FS, "tp"))
    return jax.shard_map(local, mesh=finer, in_specs=in_specs, out_specs=out_specs, check_vma=False)
```

profile of v0, /device:TPU:32, one launch (start us, length us, event | category | flops | bytes accessed | tf_op | source)
XLA Modules:
  0.0 314.9 jit_solution(17083716507183733809)
XLA Ops:
  7.2 1.2 convert_element_type.40
  10.3 19.3 %all-gather = bf16[512,704]{0,1:T(8,128)(2,1)S(1)} all-gather(bf16[128,704]{0,1:T(8,128)(2,1)S(1)} %convert_element_type.35), channel_id=2, replica_groups=mesh['rep'=2,'fs_0'=4,'fs_1'=4,'tp'=8] {'fs_0'}, dimensions={0}, use_global_device_ids=true | all-gather | bytes 901120 | tf_op jit(solution)/shard_map/all_gather | solution.py:20
  30.7 21.6 %all-gather.10.cloned.1.call-done = bf16[512,1408]{0,1:T(8,128)(2,1)} async-done(((bf16[128,1408]{0,1:T(8,128)(2,1)}), bf16[512,1408]{0,1:T(8,128)(2,1)}) %all-gather.10.cloned.1.call-update) | async-done | bytes 1441808 | tf_op jit(solution)/shard_map/all_gather | solution.py:20
  52.3 2.5 copy.27
  55.1 5.0 %fusion = bf16[2048,704]{0,1:T(8,128)(2,1)} fusion(bf16[512,2048]{1,0:T(8,128)(2,1)} %param.11, f32[704]{0:T(1024)S(1)} %reduce.1, bf16[512,704]{0,1:T(8,128)(2,1)S(1)} %copy-done.7, bf16[512,704]{0,1:T(8,128)(2,1)S(1)} %copy-done.8), kind=kOutput, calls=%fused_computation.5 | convolution fusion | flops 1482162176 | bytes 6425344 | tf_op jit(solution)/shard_map/dot_general | solution.py:96
  60.0 34.6 %all-gather.8.cloned.1.call-done = bf16[16,128,704]{1,2,0:T(8,128)(2,1)} async-done(((bf16[4,128,704]{1,2,0:T(8,128)(2,1)}), bf16[16,128,704]{1,2,0:T(8,128)(2,1)}) %all-gather.8.cloned.1.call-update) | async-done | bytes 2883600 | tf_op jit(solution)/shard_map/all_gather | solution.py:20
  94.7 5.7 %copy.26 = bf16[4,4,128,704]{2,1,0,3:T(4,128)(2,1)} copy(bf16[4,4,128,704]{2,3,0,1:T(8,128)(2,1)} %bitcast.40) | data formatting | bytes 5767168 | tf_op jit(solution)/shard_map/transpose | solution.py:23
  100.4 5.8 %reshape_reshape.6 = bf16[2048,704]{0,1:T(8,128)(2,1)} reshape(bf16[4,4,128,704]{2,1,0,3:T(4,128)(2,1)} %copy.26) | data formatting | bytes 5767168 | tf_op jit(solution)/shard_map/reshape;reshape | solution.py:14
  106.1 5.0 %fusion.6 = (bf16[512,704]{0,1:T(8,128)(2,1)S(1)}, bf16[512,704]{0,1:T(8,128)(2,1)S(1)}) fusion(bf16[512,704]{0,1:T(8,128)(2,1)S(1)} %copy-done.7, bf16[512,704]{0,1:T(8,128)(2,1)S(1)} %copy-done.8, f32[704]{0:T(1024)S(1)} %reduce.2, f32[704]{0:T(1024)S(1)} %reduce.3, f32[704]{0:T(1024)S(1)} %reduce.1, bf16[512,2048]{1,0:T(8,128)(2,1)} %param.11, ...), kind=kOutput, calls=%fused_computation.19 | convolution fusion | flops 1482883072 | bytes 7872768 | tf_op jit(solution)/shard_map/dot_general | solution.py:71
  111.1 1.7 fusion.1
  112.8 1.7 fusion.2
  114.7 4.2 %pad_maximum_fusion = bf16[2048,2112]{0,1:T(8,128)(2,1)} fusion(bf16[2048,704]{0,1:T(8,128)(2,1)S(1)} %copy-done.2, bf16[2048,704]{0,1:T(8,128)(2,1)S(1)} %fusion.2, bf16[2048,704]{0,1:T(8,128)(2,1)S(1)} %fusion.1), kind=kLoop, calls=%fused_computation | loop fusion | flops 25952256 | bytes 17301504 | tf_op jit(solution)/shard_map/concatenate | solution.py:99
  118.8 11.7 %copy.30 = bf16[2048,2112]{1,0:T(8,128)(2,1)} copy(bf16[2048,2112]{0,1:T(8,128)(2,1)} %pad_maximum_fusion) | data formatting | bytes 17301504
  130.6 30.0 %all-gather.12.cloned.1.call-done = bf16[16,128,1408]{2,1,0:T(8,128)(2,1)} async-done(((bf16[4,128,1408]{2,1,0:T(8,128)(2,1)}), bf16[16,128,1408]{2,1,0:T(8,128)(2,1)}) %all-gather.12.cloned.1.call-update) | async-done | bytes 5767184 | tf_op jit(solution)/shard_map/all_gather | solution.py:20
  160.5 3.4 %copy.28 = bf16[4,4,128,1408]{3,2,1,0:T(8,128)(2,1)S(1)} copy(bf16[4,4,128,1408]{3,2,0,1:T(8,128)(2,1)} %bitcast.37) | data formatting | bytes 11534336 | tf_op jit(solution)/shard_map/transpose | solution.py:23
  163.9 3.7 %convolution_convert_fusion.2 = bf16[512,2048]{1,0:T(8,128)(2,1)S(1)} fusion(bf16[2048,1408]{1,0:T(8,128)(2,1)S(1)} %bitcast.38, bf16[512,704]{0,1:T(8,128)(2,1)S(1)} %copy-done.12, bf16[512,704]{0,1:T(8,128)(2,1)S(1)} %copy-done.10), kind=kOutput, calls=%fused_computation.4 | convolution fusion | flops 2956722176 | bytes 9306112 | tf_op jit(solution)/shard_map/dot_general | solution.py:85
  167.7 1.5 copy.36
  169.2 4.4 %all-to-all-start = ((bf16[8,512,256]{2,1,0:T(8,128)(2,1)}), bf16[8,512,256]{2,1,0:T(8,128)(2,1)}, u32[]{:S(2)}, u32[]{:S(2)}) async-start(bf16[8,512,256]{2,1,0:T(8,128)(2,1)} %bitcast.36), calls=%async_computation | async-start | bytes 4194304 | tf_op jit(solution)/shard_map/all_to_all | solution.py:39
  173.6 94.9 %reduce-scatter.4.cloned.1.call-done = bf16[128,2112]{1,0:T(8,128)(2,1)} async-done(((bf16[2048,2112]{1,0:T(8,128)(2,1)}), bf16[128,2112]{1,0:T(8,128)(2,1)}) %reduce-scatter.4.cloned.1.call-update) | async-done | bytes 540688
  268.5 1.3 copy.31
  269.8 1.1 broadcast_in_dim.3
  270.9 7.0 %all-to-all-start.1 = ((bf16[2,128,2112]{1,2,0:T(8,128)(2,1)}), bf16[2,128,2112]{1,2,0:T(8,128)(2,1)S(1)}, u32[]{:S(2)}, u32[]{:S(2)}) async-start(bf16[2,128,2112]{1,2,0:T(8,128)(2,1)} %broadcast_in_dim.3), calls=%async_computation.1 | async-start | bytes 2162688 | tf_op jit(solution)/shard_map/all_to_all | solution.py:45
  277.9 2.8 reduce_sum.21
  280.7 26.5 %all-to-all-done.1 = bf16[2,128,2112]{1,2,0:T(8,128)(2,1)S(1)} async-done(((bf16[2,128,2112]{1,2,0:T(8,128)(2,1)}), bf16[2,128,2112]{1,2,0:T(8,128)(2,1)S(1)}, u32[]{:S(2)}, u32[]{:S(2)}) %all-to-all-start.1) | async-done | bytes 1081376 | tf_op jit(solution)/shard_map/all_to_all | solution.py:45
  (44 shorter events, 4.4 us)
Async XLA Ops:
  7.2 104.0 %copy-start = (bf16[512,2048]{1,0:T(8,128)(2,1)S(1)}, bf16[512,2048]{1,0:T(8,128)(2,1)}, u32[]{:S(2)}) copy-start(bf16[512,2048]{1,0:T(8,128)(2,1)} %param.10) | copy-start | bytes 6291460
  7.2 3.1 copy-start.3
  7.2 45.1 %all-gather.10.cloned.1.call-start = ((), (), s32[]{:S(2)}) async-start(), calls=%async_computation.4 | async-start | bytes 1802240 | tf_op jit(solution)/shard_map/all_gather | solution.py:20
  10.2 84.5 %all-gather.8.cloned.1.call-start = ((), (), s32[]{:S(2)}) async-start(), calls=%async_computation.3 | async-start | bytes 3604480 | tf_op jit(solution)/shard_map/all_gather | solution.py:20
  30.6 24.4 %copy-start.4 = (f32[1,704]{1,0:T(1,128)S(1)}, f32[1,704]{1,0:T(1,128)}, u32[]{:S(2)}) copy-start(f32[1,704]{1,0:T(1,128)} %param.19) | copy-start | bytes 8452
  30.6 24.4 %copy-start.5 = (f32[1,704]{1,0:T(1,128)S(1)}, f32[1,704]{1,0:T(1,128)}, u32[]{:S(2)}) copy-start(f32[1,704]{1,0:T(1,128)} %param.17) | copy-start | bytes 8452
  30.6 24.4 %copy-start.6 = (f32[1,704]{1,0:T(1,128)S(1)}, f32[1,704]{1,0:T(1,128)}, u32[]{:S(2)}) copy-start(f32[1,704]{1,0:T(1,128)} %param.18) | copy-start | bytes 8452
  30.6 24.4 %copy-start.7 = (bf16[512,704]{0,1:T(8,128)(2,1)S(1)}, bf16[512,704]{0,1:T(8,128)(2,1)}, u32[]{:S(2)}) copy-start(bf16[512,704]{0,1:T(8,128)(2,1)} %param.13) | copy-start | bytes 2162692
  30.6 24.4 %copy-start.8 = (bf16[512,704]{0,1:T(8,128)(2,1)S(1)}, bf16[512,704]{0,1:T(8,128)(2,1)}, u32[]{:S(2)}) copy-start(bf16[512,704]{0,1:T(8,128)(2,1)} %param.12) | copy-start | bytes 2162692
  30.6 129.9 %all-gather.12.cloned.1.call-start = ((), (), s32[]{:S(2)}) async-start(), calls=%async_computation.5 | async-start | bytes 7208960 | tf_op jit(solution)/shard_map/all_gather | solution.py:20
  54.9 213.6 %reduce-scatter.4.cloned.1.call-start = ((), (), s32[]{:S(2)}) async-start(), calls=%async_computation.6 | async-start | bytes 9469952
  111.1 1.7 copy-start.9
  111.1 1.7 copy-start.11
  112.8 1.8 copy-start.2
  160.5 3.4 %copy-start.10 = (bf16[512,704]{0,1:T(8,128)(2,1)S(1)}, bf16[512,704]{0,1:T(8,128)(2,1)}, u32[]{:S(2)}) copy-start(bf16[512,704]{0,1:T(8,128)(2,1)} %copy-done.9) | copy-start | bytes 2162692
  160.5 3.4 %copy-start.12 = (bf16[512,704]{0,1:T(8,128)(2,1)S(1)}, bf16[512,704]{0,1:T(8,128)(2,1)}, u32[]{:S(2)}) copy-start(bf16[512,704]{0,1:T(8,128)(2,1)} %copy-done.11) | copy-start | bytes 2162692
  169.2 100.6 %all-to-all-start = ((bf16[8,512,256]{2,1,0:T(8,128)(2,1)}), bf16[8,512,256]{2,1,0:T(8,128)(2,1)}, u32[]{:S(2)}, u32[]{:S(2)}) async-start(bf16[8,512,256]{2,1,0:T(8,128)(2,1)} %bitcast.36), calls=%async_computation | async-start | bytes 4194304 | tf_op jit(solution)/shard_map/all_to_all | solution.py:39
  270.9 36.3 %all-to-all-start.1 = ((bf16[2,128,2112]{1,2,0:T(8,128)(2,1)}), bf16[2,128,2112]{1,2,0:T(8,128)(2,1)S(1)}, u32[]{:S(2)}, u32[]{:S(2)}) async-start(bf16[2,128,2112]{1,2,0:T(8,128)(2,1)} %broadcast_in_dim.3), calls=%async_computation.1 | async-start | bytes 2162688 | tf_op jit(solution)/shard_map/all_to_all | solution.py:45
  277.9 30.5 %copy-start.1 = (bf16[512,2048]{1,0:T(8,128)(2,1)S(1)}, bf16[512,2048]{1,0:T(8,128)(2,1)}, u32[]{:S(2)}) copy-start(bf16[512,2048]{1,0:T(8,128)(2,1)} %param.10) | copy-start | bytes 6291460
Sparse Core Ops, SparseCore 0:
  10.4 41.9 all-gather.9
  54.1 40.5 all-gather.7
  96.5 63.9 all-gather.11
  163.0 105.4 reduce-scatter.3
where the time goes:
time: 316 us; the launch traced here: 315 us
  waiting for transfers between devices  208 us (66%)
  local copies, waits for them, and re-layouts  35.2 us (11%)
  blocking collectives  19.3 us (6%)
  matrix products  17 us (5%)
  between operations  14 us (4%)
  starting transfers between devices  11.5 us (4%)
  other arithmetic  10.1 us (3%)
    unnamed x5, waiting for transfers between devices  95 us
    all_gather x3, waiting for transfers between devices, stacked_from(): parts = lax.all_gather(parts, axes[k])  86.2 us
    all_to_all x1, waiting for transfers between devices, copy_for_each(): return lax.all_to_all(copies, axis, split_axis=0, concat_axis=0, tiled=True)  26.5 us
    all_gather x1, blocking collectives, stacked_from(): parts = lax.all_gather(parts, axes[k])  19.3 us
    unnamed x28, local copies, waits for them, and re-layouts  13.3 us
    transpose x2, local copies, waits for them, and re-layouts, stacked_from(): parts = parts.transpose(*back, *range(len(axes), parts.ndim))  9.04 us
    all_to_all x1, starting transfers between devices, copy_for_each(): return lax.all_to_all(copies, axis, split_axis=0, concat_axis=0, tiled=True)  7 us
  transfers between devices with their start and end apart: 6, of which 5 were waited for; matrix products, arithmetic and copies ran while one was open for 18% of the time, Pallas kernels for 0%

commit v1 on v0

v1 whole, which is shorter than its diff:
```python
import jax
import jax.numpy as jnp
from jax import lax
from jax.experimental import pallas as pl
from jax.experimental.pallas import tpu as pltpu
from jax.sharding import PartitionSpec as P

MESH = pl.DeviceIdType.MESH
F32 = jnp.float32
BF16 = jnp.bfloat16
ROWS = 128
HALF = 64
TOK = 512
D = 2048
FFL = 704
GU = 1408
MAIN = 640
NTP = 8


def kernel(
    x_hbm, cot_hbm, gate_hbm, up_hbm, wd_hbm, wgu_hbm, gs_ref, us_ref, ds_ref,
    oi_ref, og_ref, ou_ref, od_ref,
    x, cot, gate, up, hidden, fg, fu, bc,
    wd, wgu, gd, ggu,
    d_r1, d_r2, d_s, d_b1, d_b2, d_f, d_q1, d_q2,
    g_r1, g_r2, g_s, g_b1, g_b2, g_f, g_q1, g_q2,
    tp_out, tp_in,
    local_sem, ag_send, ag_recv, rs_send, rs_recv, tp_send, tp_recv,
):
    rep = lax.axis_index("rep")
    fs = lax.axis_index("fs")
    tp = lax.axis_index("tp")
    y = lax.rem(fs, 4)
    zl = lax.div(fs, 4)
    z = rep * 4 + zl

    def near(dy, dz):
        yy = lax.rem(y + dy + 4, 4)
        zz = lax.rem(z + dz + 8, 8)
        return (lax.div(zz, 4), lax.rem(zz, 4) * 4 + yy, tp)

    def tp_peer(r):
        return (rep, fs, lax.rem(tp + r, NTP))

    def yi(k):
        return lax.rem(y + k + 4, 4)

    def zi(k):
        return lax.rem(zl + k + 4, 4)

    loads = {}
    for k, (src, dst) in enumerate(
        (
            (wd_hbm, wd.at[zl, y]),
            (wgu_hbm, wgu.at[zl, y]),
            (gate_hbm, gate),
            (up_hbm, up),
            (cot_hbm, cot),
            (x_hbm, x),
        )
    ):
        loads[k] = pltpu.make_async_copy(src, dst, local_sem.at[k])
        loads[k].start()

    barrier = pltpu.get_barrier_semaphore()
    peers = [near(1, 0), near(3, 0), near(0, 1), near(0, 7), near(0, 2), near(0, 6)]
    peers += [tp_peer(r) for r in range(1, NTP)]
    for peer in peers:
        pl.semaphore_signal(barrier, inc=1, device_id=peer, device_id_type=MESH)
    loads[0].wait()
    loads[1].wait()
    pl.semaphore_wait(barrier, len(peers))

    sends = []

    def remote(src, dst, send_sem, recv_sem, peer):
        return pltpu.make_async_remote_copy(
            src_ref=src, dst_ref=dst, send_sem=send_sem, recv_sem=recv_sem,
            device_id=peer, device_id_type=MESH,
        )

    AGN = 20

    class Gather:
        def __init__(self, buf, base, first_z):
            self.buf, self.base, self.first_z = buf, base, first_z

        def blk(self, ia, ib):
            if self.first_z:
                return self.buf.at[zi(ia), yi(ib)]
            return self.buf.at[zi(ib), yi(ia)]

        def half(self, ia, ib, h):
            rows = pl.ds(h * HALF, HALF)
            if self.first_z:
                return self.buf.at[zi(ia), yi(ib), rows]
            return self.buf.at[zi(ib), yi(ia), rows]

        def peer_a(self, s):
            return near(0, s) if self.first_z else near(s, 0)

        def peer_b(self, s):
            return near(s, 0) if self.first_z else near(0, s)

        def send(self, k, ref, peer):
            c = remote(ref, ref, ag_send.at[self.base + k], ag_recv.at[self.base + k], peer)
            c.start()
            sends.append(c)

        def got(self, k, ref):
            remote(
                ref, ref, ag_send.at[self.base + k], ag_recv.at[self.base + k], near(1, 0)
            ).wait_recv()

        def own_a(self):
            self.send(0, self.blk(0, 0), self.peer_a(1))
            self.send(1, self.blk(0, 0), self.peer_a(-1))

        def to_b(self, k, ia):
            self.send(k, self.blk(ia, 0), self.peer_b(1))
            self.send(k + 1, self.blk(ia, 0), self.peer_b(-1))

        def own_b(self):
            self.to_b(2, 0)

        def recv_a(self):
            self.got(0, self.blk(-1, 0))
            self.send(4, self.half(-1, 0, 0), self.peer_a(1))
            self.to_b(6, -1)
            self.got(1, self.blk(1, 0))
            self.send(5, self.half(1, 0, 1), self.peer_a(-1))
            self.to_b(8, 1)

        def recv_far(self):
            self.got(4, self.half(2, 0, 0))
            self.got(5, self.half(2, 0, 1))
            self.to_b(10, 2)

        def recv_b(self, n):
            ia = (0, -1, 1, 2)[n]
            k = (2, 6, 8, 10)[n]
            self.got(k, self.blk(ia, -1))
            self.send(12 + 2 * n, self.half(ia, -1, 0), self.peer_b(1))
            self.got(k + 1, self.blk(ia, 1))
            self.send(13 + 2 * n, self.half(ia, 1, 1), self.peer_b(-1))

        def last(self):
            for n in range(4):
                ia = (0, -1, 1, 2)[n]
                self.got(12 + 2 * n, self.half(ia, 2, 0))
                self.got(13 + 2 * n, self.half(ia, 2, 1))

    def add_rows(n, fn):
        @pl.loop(0, n // 16)
        def _(i):
            fn(pl.ds(pl.multiple_of(i * 16, 16), 16))

    class Reduce:
        def __init__(self, grad, r1, r2, s, b1, b2, f, q1, q2, base, first_z):
            self.grad, self.r1, self.r2, self.s = grad, r1, r2, s
            self.b1, self.b2, self.f, self.q1, self.q2 = b1, b2, f, q1, q2
            self.base, self.first_z = base, first_z

        def part(self, ia, h):
            if self.first_z:
                return self.grad.at[zi(ia), pl.ds(2 * h, 2)]
            return self.grad.at[pl.ds(2 * h, 2), yi(ia)]

        def ib(self, k):
            return yi(k) if self.first_z else zi(k)

        def peer_a(self, s):
            return near(0, s) if self.first_z else near(s, 0)

        def peer_b(self, s):
            return near(s, 0) if self.first_z else near(0, s)

        def send(self, k, src, dst, peer):
            c = remote(src, dst, rs_send.at[self.base + k], rs_recv.at[self.base + k], peer)
            c.start()
            sends.append(c)

        def got(self, k, ref):
            remote(
                ref, ref, rs_send.at[self.base + k], rs_recv.at[self.base + k], near(1, 0)
            ).wait_recv()

        def start_far(self, h):
            if h == 0:
                self.send(0, self.part(2, 0), self.r1.at[0], self.peer_a(1))
            else:
                self.send(1, self.part(2, 1), self.r1.at[1], self.peer_a(-1))

        def start_plus(self):
            self.send(2, self.part(1, 1), self.r2.at[0, pl.ds(2, 2)], self.peer_a(1))

        def start_minus(self):
            self.send(3, self.part(-1, 0), self.r2.at[1, pl.ds(0, 2)], self.peer_a(-1))

        def acc_part(self, ia, h, inc):
            for j in range(2):
                def body(rows, j=j):
                    if self.first_z:
                        at = (zi(ia), 2 * h + j, rows)
                    else:
                        at = (2 * h + j, yi(ia), rows)
                    total = self.grad[at].astype(F32) + inc[j, rows].astype(F32)
                    self.grad[at] = total.astype(BF16)

                add_rows(ROWS, body)

        def pass_on(self):
            self.got(0, self.r1.at[0])
            self.acc_part(1, 0, self.r1.at[0])
            self.send(4, self.part(1, 0), self.r2.at[0, pl.ds(0, 2)], self.peer_a(1))
            self.got(1, self.r1.at[1])
            self.acc_part(-1, 1, self.r1.at[1])
            self.send(5, self.part(-1, 1), self.r2.at[1, pl.ds(2, 2)], self.peer_a(-1))

        def gather_own(self):
            self.got(2, self.r2.at[0, pl.ds(2, 2)])
            self.got(3, self.r2.at[1, pl.ds(0, 2)])
            self.got(4, self.r2.at[0, pl.ds(0, 2)])
            self.got(5, self.r2.at[1, pl.ds(2, 2)])
            self.sum_own(2)
            self.send(6, self.s.at[self.ib(2), pl.ds(0, HALF)], self.b1.at[0], self.peer_b(1))
            self.send(7, self.s.at[self.ib(2), pl.ds(HALF, HALF)], self.b1.at[1], self.peer_b(-1))
            self.sum_own(1)
            self.send(
                8, self.s.at[self.ib(1), pl.ds(HALF, HALF)],
                self.b2.at[0, pl.ds(HALF, HALF)], self.peer_b(1),
            )
            self.sum_own(-1)
            self.send(
                9, self.s.at[self.ib(-1), pl.ds(0, HALF)],
                self.b2.at[1, pl.ds(0, HALF)], self.peer_b(-1),
            )
            self.sum_own(0)

        def sum_own(self, k):
            ib = self.ib(k)

            def body(rows):
                at = (zi(0), ib, rows) if self.first_z else (ib, yi(0), rows)
                total = self.grad[at].astype(F32) + self.r2[0, ib, rows].astype(F32)
                total = total + self.r2[1, ib, rows].astype(F32)
                self.s[ib, rows] = total.astype(BF16)

            add_rows(ROWS, body)

        def pass_on_b(self):
            self.got(6, self.b1.at[0])

            def plus(rows):
                total = self.s[self.ib(1), rows].astype(F32) + self.b1[0, rows].astype(F32)
                self.s[self.ib(1), rows] = total.astype(BF16)

            add_rows(HALF, plus)
            self.send(
                10, self.s.at[self.ib(1), pl.ds(0, HALF)],
                self.b2.at[0, pl.ds(0, HALF)], self.peer_b(1),
            )
            self.got(7, self.b1.at[1])

            @pl.loop(0, HALF // 16)
            def _(i):
                low = pl.ds(pl.multiple_of(i * 16, 16), 16)
                rows = pl.ds(pl.multiple_of(HALF + i * 16, 16), 16)
                total = self.s[self.ib(-1), rows].astype(F32) + self.b1[1, low].astype(F32)
                self.s[self.ib(-1), rows] = total.astype(BF16)

            self.send(
                11, self.s.at[self.ib(-1), pl.ds(HALF, HALF)],
                self.b2.at[1, pl.ds(HALF, HALF)], self.peer_b(-1),
            )

        def finish_b(self):
            self.got(8, self.b2.at[0, pl.ds(HALF, HALF)])
            self.got(9, self.b2.at[1, pl.ds(0, HALF)])
            self.got(10, self.b2.at[0, pl.ds(0, HALF)])
            self.got(11, self.b2.at[1, pl.ds(HALF, HALF)])

            def body(rows):
                total = self.s[self.ib(0), rows].astype(F32) + self.b2[0, rows].astype(F32)
                total = total + self.b2[1, rows].astype(F32)
                self.f[rows] = total.astype(BF16)

            add_rows(ROWS, body)
            self.send(12, self.f.at[pl.ds(0, HALF)], self.q1.at[0], near(0, 2))
            self.send(13, self.f.at[pl.ds(HALF, HALF)], self.q1.at[1], near(0, -2))

        def relay(self):
            self.got(12, self.q1.at[0])
            self.send(14, self.q1.at[0], self.q2.at[pl.ds(0, HALF)], near(0, 2))
            self.got(13, self.q1.at[1])
            self.send(15, self.q1.at[1], self.q2.at[pl.ds(HALF, HALF)], near(0, -2))

        def arrive(self):
            self.got(14, self.q2.at[pl.ds(0, HALF)])
            self.got(15, self.q2.at[pl.ds(HALF, HALF)])

    ag_d = Gather(wd, 0, True)
    ag_g = Gather(wgu, AGN, False)
    rs_d = Reduce(gd, d_r1, d_r2, d_s, d_b1, d_b2, d_f, d_q1, d_q2, 0, True)
    rs_g = Reduce(ggu, g_r1, g_r2, g_s, g_b1, g_b2, g_f, g_q1, g_q2, 16, False)

    ag_d.own_a()
    ag_d.own_b()
    ag_g.own_a()
    ag_g.own_b()

    loads[2].wait()
    loads[3].wait()

    @pl.loop(0, TOK // 16)
    def _(i):
        rows = pl.ds(pl.multiple_of(i * 16, 16), 16)
        g = gate[rows, :].astype(F32)
        u = up[rows, :].astype(F32)
        sig = jax.nn.sigmoid(g)
        act = g * sig
        hidden[rows, :] = (act * u).astype(BF16)
        down = ds_ref[...]
        fg[rows, :] = u * sig * (1.0 + g * (1.0 - sig)) * (gs_ref[...] * down)
        fu[rows, :] = act * (us_ref[...] * down)

    ag_d.recv_a()
    ag_g.recv_a()
    ag_d.recv_b(0)
    ag_d.recv_far()
    ag_g.recv_b(0)

    loads[4].wait()

    def down_slab(k):
        zz = zi(k)
        for j in range(2):
            cols = pl.ds(pl.multiple_of(zz * 512 + j * 256, 256), 256)
            out = lax.dot_general(
                cot[:, cols], hidden[...], (((0,), (0,)), ((), ())), preferred_element_type=F32
            ).astype(BF16)
            gd[zz, 2 * j] = out[:ROWS]
            gd[zz, 2 * j + 1] = out[ROWS:]

    @pl.loop(0, 4)
    def _(k):
        zz = k
        for j in range(2):
            cols = pl.ds(pl.multiple_of(zz * 512 + j * 256, 256), 256)
            out = lax.dot_general(
                cot[:, cols], hidden[...], (((0,), (0,)), ((), ())), preferred_element_type=F32
            ).astype(BF16)
            gd[zz, 2 * j] = out[:ROWS]
            gd[zz, 2 * j + 1] = out[ROWS:]

    ag_g.recv_far()
    ag_d.recv_b(1)
    ag_d.recv_b(2)
    ag_g.recv_b(1)
    ag_d.recv_b(3)
    ag_g.recv_b(2)
    ag_d.last()

    @pl.loop(0, 2)
    def _(m):
        rows = pl.ds(pl.multiple_of(m * 256, 256), 256)
        hc = jnp.dot(
            cot[rows, :], wd[...].reshape(D, FFL), preferred_element_type=F32
        )
        gc = (hc * fg[rows, :]).astype(BF16)
        uc = (hc * fu[rows, :]).astype(BF16)
        bc[rows, pl.ds(0, MAIN)] = gc[:, :MAIN]
        bc[rows, pl.ds(MAIN, MAIN)] = uc[:, :MAIN]
        bc[rows, pl.ds(2 * MAIN, 128)] = jnp.concatenate([gc[:, MAIN:], uc[:, MAIN:]], axis=1)

    ag_g.recv_b(3)
    rs_d.start_far(0)
    rs_d.start_far(1)
    rs_d.start_plus()
    rs_d.start_minus()
    loads[5].wait()

    @pl.loop(0, 4)
    def _(k):
        yy = lax.rem(y + 2 + k, 4)
        for j in range(2):
            lo = pl.ds(pl.multiple_of((8 * j + yy) * ROWS, ROWS), ROWS)
            hi = pl.ds(pl.multiple_of((8 * j + 4 + yy) * ROWS, ROWS), ROWS)
            both = jnp.concatenate([x[:, lo], x[:, hi]], axis=1)
            out = lax.dot_general(
                both, bc[...], (((0,), (0,)), ((), ())), preferred_element_type=F32
            ).astype(BF16)
            ggu[2 * j, yy] = out[:ROWS]
            ggu[2 * j + 1, yy] = out[ROWS:]

    rs_g.start_far(0)
    rs_g.start_far(1)
    rs_g.start_plus()
    rs_g.start_minus()

    ag_g.last()

    @pl.loop(0, NTP)
    def _(r):
        t = lax.rem(tp + r, NTP)
        w = wgu[lax.div(t, 2), pl.ds(lax.rem(t, 2) * 2, 2)].reshape(256, GU)
        part = lax.dot_general(
            bc[...], w, (((1,), (1,)), ((), ())), preferred_element_type=F32
        )
        tp_out[r] = part.astype(BF16)

    for r in range(1, NTP):
        c = remote(tp_out.at[r], tp_in.at[r], tp_send.at[r], tp_recv.at[r], tp_peer(r))
        c.start()
        sends.append(c)

    rs_d.pass_on()
    rs_g.pass_on()
    rs_d.gather_own()
    rs_d.pass_on_b()
    rs_d.finish_b()
    rs_d.relay()
    rs_g.gather_own()
    rs_g.pass_on_b()
    rs_g.finish_b()
    rs_d.arrive()

    def down_out(rows):
        total = d_f[rows].astype(F32) + d_q2[rows].astype(F32)
        od_ref[rows, :] = total * ds_ref[...]

    add_rows(ROWS, down_out)

    for r in range(1, NTP):
        remote(
            tp_in.at[r], tp_in.at[r], tp_send.at[r], tp_recv.at[r], tp_peer(r)
        ).wait_recv()

    def input_out(rows):
        total = tp_out[0, rows].astype(F32)
        for r in range(1, NTP):
            total = total + tp_in[r, rows].astype(F32)
        oi_ref[rows, :] = total.astype(BF16)

    add_rows(TOK, input_out)

    rs_g.relay()
    rs_g.arrive()

    def gate_up_out(rows):
        total = g_f[rows].astype(F32) + g_q2[rows].astype(F32)
        og_ref[rows, pl.ds(0, MAIN)] = total[:, :MAIN]
        ou_ref[rows, pl.ds(0, MAIN)] = total[:, MAIN : 2 * MAIN]
        og_ref[rows, pl.ds(MAIN, HALF)] = total[:, 2 * MAIN : 2 * MAIN + HALF]
        ou_ref[rows, pl.ds(MAIN, HALF)] = total[:, 2 * MAIN + HALF :]

    add_rows(ROWS, gate_up_out)

    for c in sends:
        c.wait_send()


def reduce_scratch(c):
    return [
        pltpu.VMEM((2, 2, ROWS, c), BF16),
        pltpu.VMEM((2, 4, ROWS, c), BF16),
        pltpu.VMEM((4, ROWS, c), BF16),
        pltpu.VMEM((2, HALF, c), BF16),
        pltpu.VMEM((2, ROWS, c), BF16),
        pltpu.VMEM((ROWS, c), BF16),
        pltpu.VMEM((2, HALF, c), BF16),
        pltpu.VMEM((ROWS, c), BF16),
    ]


def local(
    inputs, cotangent, gate_pre, up_pre, gate_weight, up_weight, down_weight,
    gate_scale, up_scale, down_scale,
):
    wd = down_weight.astype(BF16)
    wgu = jnp.concatenate(
        [gate_weight[:, :MAIN], up_weight[:, :MAIN], gate_weight[:, MAIN:], up_weight[:, MAIN:]],
        axis=1,
    ).astype(BF16)
    hbm = pl.BlockSpec(memory_space=pl.ANY)
    vmem = pl.BlockSpec(memory_space=pltpu.VMEM)
    return pl.pallas_call(
        kernel,
        out_shape=(
            jax.ShapeDtypeStruct((TOK, 256), BF16),
            jax.ShapeDtypeStruct((ROWS, FFL), F32),
            jax.ShapeDtypeStruct((ROWS, FFL), F32),
            jax.ShapeDtypeStruct((ROWS, FFL), F32),
        ),
        in_specs=[hbm] * 6 + [vmem] * 3,
        out_specs=(vmem,) * 4,
        scratch_shapes=[
            pltpu.VMEM((TOK, D), BF16),
            pltpu.VMEM((TOK, D), BF16),
            pltpu.VMEM((TOK, FFL), BF16),
            pltpu.VMEM((TOK, FFL), BF16),
            pltpu.VMEM((TOK, FFL), BF16),
            pltpu.VMEM((TOK, FFL), F32),
            pltpu.VMEM((TOK, FFL), F32),
            pltpu.VMEM((TOK, GU), BF16),
            pltpu.VMEM((4, 4, ROWS, FFL), BF16),
            pltpu.VMEM((4, 4, ROWS, GU), BF16),
            pltpu.VMEM((4, 4, ROWS, FFL), BF16),
            pltpu.VMEM((4, 4, ROWS, GU), BF16),
            *reduce_scratch(FFL),
            *reduce_scratch(GU),
            pltpu.VMEM((NTP, TOK, 256), BF16),
            pltpu.VMEM((NTP, TOK, 256), BF16),
            pltpu.SemaphoreType.DMA((6,)),
            pltpu.SemaphoreType.DMA((40,)),
            pltpu.SemaphoreType.DMA((40,)),
            pltpu.SemaphoreType.DMA((32,)),
            pltpu.SemaphoreType.DMA((32,)),
            pltpu.SemaphoreType.DMA((NTP,)),
            pltpu.SemaphoreType.DMA((NTP,)),
        ],
        compiler_params=pltpu.CompilerParams(
            collective_id=0, has_side_effects=True, vmem_limit_bytes=60 * 1024 * 1024
        ),
    )(inputs, cotangent, gate_pre, up_pre, wd, wgu, gate_scale, up_scale, down_scale)


def solution(mesh):
    rows = ("rep", "fs")
    in_specs = (
        P(rows, None), P(rows, None), P(rows, "tp"), P(rows, "tp"),
        P("fs", "tp"), P("fs", "tp"), P("fs", "tp"),
        P(None, "tp"), P(None, "tp"), P(None, "tp"),
    )
    out_specs = (P(rows, "tp"), P("fs", "tp"), P("fs", "tp"), P("fs", "tp"))
    return jax.shard_map(local, mesh=mesh, in_specs=in_specs, out_specs=out_specs, check_vma=False)
```

time: 316 us -> 173 us (0.55)
  waiting for transfers between devices: 208 us -> 0 us
  Pallas kernels: 0 us -> 156 us
  local copies, waits for them, and re-layouts: 35.2 us -> 14.7 us
  blocking collectives: 19.3 us -> 0 us
  matrix products: 17 us -> 0 us
  between operations: 14 us -> 0.69 us
  starting transfers between devices: 11.5 us -> 0 us
  other arithmetic: 10.1 us -> 0.02 us
    pallas_call x0 -> x1, Pallas kernels: none -> 156 us  [local(): pl.pallas_call(kernel, out_shape=(jax.ShapeDtypeStruct((TOK, 256), BF16),...]
    unnamed x5 -> x0, waiting for transfers between devices: 95 us -> none
    all_gather x3 -> x0, waiting for transfers between devices: 86.2 us -> none  [stacked_from(): parts = lax.all_gather(parts, axes[k])]
    all_to_all x2 -> x0, waiting for transfers between devices: 26.5 us -> none  [the longest x1 26.5 us: copy_for_each(): return lax.all_to_all(copies, axis, split_axis=0, concat_axis=0, tiled=True)]
    all_gather x1 -> x0, blocking collectives: 19.3 us -> none  [stacked_from(): parts = lax.all_gather(parts, axes[k])]
    dot_general x5 -> x0, matrix products: 17 us -> none  [the longest x1 4.99 us: local(): lax.dot_general(cotangent, hidden, dims, preferred_element_type=jnp.float32)]
    all_to_all x2 -> x0, starting transfers between devices: 11.4 us -> none  [the longest x1 7 us: copy_for_each(): return lax.all_to_all(copies, axis, split_axis=0, concat_axis=0, tiled=True)]
    unnamed x28 -> x15, local copies, waits for them, and re-layouts: 13.3 us -> 3.61 us
  transfers between devices with their start and end apart: 6 -> 0, of which waited for: 5 -> 0; matrix products, arithmetic and copies ran while one was open for 18% -> 0% of each run, Pallas kernels for 0% -> 0%
where the time goes in v1:
time: 173 us; the launch traced here: 171 us
  Pallas kernels  156 us (90%)
  local copies, waits for them, and re-layouts  14.7 us (8%)
    pallas_call x1, Pallas kernels, local(): pl.pallas_call(kernel, out_shape=(jax.ShapeDtypeStruct((TOK, 256), BF16),...  156 us
    pallas_call x3, local copies, waits for them, and re-layouts, local(): pl.pallas_call(kernel, out_shape=(jax.ShapeDtypeStruct((TOK, 256), BF16),...  5.74 us
    unnamed x15, local copies, waits for them, and re-layouts  3.61 us

profile of v1, /device:TPU:32, one launch (start us, length us, event | category | flops | bytes accessed | tf_op | source)
XLA Modules:
  0.0 171.4 jit_solution(11521835728014036385)
XLA Ops:
  0.6 0.0 copy-start.2
  0.6 0.0 copy-start
  0.7 0.9 slice.22
  1.5 0.1 copy.32
  1.6 0.8 slice.23
  2.4 0.1 copy.33
  2.5 1.0 slice.20
  3.5 0.0 copy-start.1
  3.5 0.2 copy.30
  3.7 1.0 slice.21
  4.7 0.2 copy.31
  4.9 0.8 concatenate.4.wgu_hbm
  5.7 0.0 copy-done.2
  5.7 0.8 copy.26.wd_hbm
  6.6 0.0 copy-done
  6.6 1.2 copy.24.gate_hbm
  7.7 0.0 copy-done.1
  7.7 1.2 copy.25.up_hbm
  8.9 156.0 %shard_map.129 = (bf16[512,256]{1,0:T(8,128)(2,1)}, f32[128,704]{1,0:T(8,128)}, f32[128,704]{1,0:T(8,128)}, f32[128,704]{1,0:T(8,128)}) custom-call(bf16[512,2048]{1,0:T(8,128)(2,1)} %x_hbm.1, bf16[512,2048]{1,0:T(8,128)(2,1)} %cot_hbm.1, bf16[512,704]{1,0:T(8,128)(2,1)} %copy.24.gate_hbm, bf16[512,704]{1,0:T(8,128)(2,1)} %copy.25.up_hbm, ...), custom_call_target="tpu_custom_call" | custom-call | tf_op jit(solution)/shard_map/pallas_call | solution.py:488
  164.9 0.0 copy-start.3
  164.9 1.9 %copy.27 = f32[128,704]{0,1:T(8,128)} copy(f32[128,704]{1,0:T(8,128)} %get-tuple-element.9) | data formatting | bytes 720896 | tf_op jit(solution)/shard_map/pallas_call | solution.py:488
  166.9 1.9 %copy.28 = f32[128,704]{0,1:T(8,128)} copy(f32[128,704]{1,0:T(8,128)} %get-tuple-element.10) | data formatting | bytes 720896 | tf_op jit(solution)/shard_map/pallas_call | solution.py:488
  168.8 1.9 %copy.29 = f32[128,704]{0,1:T(8,128)} copy(f32[128,704]{1,0:T(8,128)} %get-tuple-element.11) | data formatting | bytes 720896 | tf_op jit(solution)/shard_map/pallas_call | solution.py:488
  170.7 0.7 copy.35
  (2 shorter events, 0.0 us)
Async XLA Ops:
  0.6 5.1 %copy-start.2 = (f32[128,704]{0,1:T(8,128)S(1)}, f32[128,704]{0,1:T(8,128)}, u32[]{:S(2)}) copy-start(f32[128,704]{0,1:T(8,128)} %param.16) | copy-start | bytes 1081348
  0.6 5.9 %copy-start = (bf16[512,704]{0,1:T(8,128)(2,1)S(1)}, bf16[512,704]{0,1:T(8,128)(2,1)}, u32[]{:S(2)}) copy-start(bf16[512,704]{0,1:T(8,128)(2,1)} %param.12) | copy-start | bytes 2162692
  3.5 4.2 %copy-start.1 = (bf16[512,704]{0,1:T(8,128)(2,1)S(1)}, bf16[512,704]{0,1:T(8,128)(2,1)}, u32[]{:S(2)}) copy-start(bf16[512,704]{0,1:T(8,128)(2,1)} %param.13) | copy-start | bytes 2162692
  164.9 5.7 %copy-start.3 = (bf16[512,256]{1,0:T(8,128)(2,1)S(1)}, bf16[512,256]{1,0:T(8,128)(2,1)}, u32[]{:S(2)}) copy-start(bf16[512,256]{1,0:T(8,128)(2,1)} %get-tuple-element.16) | copy-start | bytes 786436

commit v2 on v0

v2 whole, which is shorter than its diff:
```python
import jax
import jax.numpy as jnp
from jax import lax
from jax.experimental import pallas as pl
from jax.experimental.pallas import tpu as pltpu
from jax.sharding import PartitionSpec as P

MESH = pl.DeviceIdType.MESH
F32 = jnp.float32
BF16 = jnp.bfloat16
LANES = 128
TOK = 512
D = 2048
FFL = 704
GU = 2 * FFL
ALL = 3 * FFL
NTP = 8

PIECES = (
    ("d", 0, 704, True, True),
    ("g", 704, 704, False, False),
    ("u", 1408, 704, True, True),
)
ORDER = (
    "ag0 g", "ag0 d", "ew", "a1 g", "b0+ g", "b0- g", "a0 g", "a1 d", "b0- d", "b0+ d", "a0 d",
    "far g", "b2+ g", "b2- g", "b2+ d", "b2- d", "ag0 u", "b1- g", "b1+ g", "far d", "b1+ d",
    "b1- d", "b3+ g", "b3- g", "b0- u", "b0+ u", "a1 u", "a0 u", "b3+ d", "b3- d", "down",
    "rs0 d", "last g", "far u", "b2+ u", "b2- u", "b1- u", "b1+ u", "p0 d", "last d", "p1 d",
    "hc", "b3+ u", "b3- u", "gu", "rs0 u", "rs0 g", "last u", "part", "p1 g", "p0 g", "p0 u",
    "p1 u", "own d", "own g", "q1 d", "q0 d", "own u", "q0 g", "q1 g", "fin d", "q1 u", "q0 u",
    "fin g", "fin u", "y0 d", "y1 d", "tp", "y0 g", "y1 g", "y0 u", "y1 u", "arr d", "arr g",
    "arr u",
)

def kernel(
    x_hbm, cot_hbm, gate_hbm, up_hbm, wd_hbm, wg_hbm, wu_hbm, gs_ref, us_ref, ds_ref,
    oi_ref, og_ref, ou_ref, od_ref,
    x, cot, gate, up, w32, scales, hidden, fg, fu, bc,
    w, grad, r1, r2, own, b1, b2, final, q1, q2,
    tp_out, tp_in,
    local_sem, ag_send, ag_recv, rs_send, rs_recv, tp_send, tp_recv,
):
    rep = lax.axis_index("rep")
    fs = lax.axis_index("fs")
    tp = lax.axis_index("tp")
    y = lax.rem(fs, 4)
    zl = lax.div(fs, 4)
    z = rep * 4 + zl

    def near(dy, dz):
        yy = lax.rem(y + dy + 4, 4)
        zz = lax.rem(z + dz + 8, 8)
        return (lax.div(zz, 4), lax.rem(zz, 4) * 4 + yy, tp)

    def tp_peer(r):
        return (rep, fs, lax.rem(tp + r, NTP))

    def yi(k):
        return lax.rem(y + k + 4, 4)

    def zi(k):
        return lax.rem(zl + k + 4, 4)

    def chunks(n, fn):
        @pl.loop(0, n // 32)
        def _(i):
            fn(i * 32)

    def rows32(start):
        return pl.ds(pl.multiple_of(start, 16), 32)

    loads = []
    for k, (src, dst) in enumerate(
        (
            (wd_hbm, w32.at[pl.ds(0, FFL)]),
            (wg_hbm, w32.at[pl.ds(FFL, FFL)]),
            (wu_hbm, w32.at[pl.ds(GU, FFL)]),
            (gate_hbm, gate),
            (up_hbm, up),
            (cot_hbm, cot),
            (x_hbm, x),
        )
    ):
        loads.append(pltpu.make_async_copy(src, dst, local_sem.at[k]))
        loads[k].start()

    barrier = pltpu.get_barrier_semaphore()
    peers = [near(1, 0), near(3, 0), near(0, 1), near(0, 7), near(0, 2), near(0, 6)]
    peers += [tp_peer(r) for r in range(1, NTP)]
    for peer in peers:
        pl.semaphore_signal(barrier, inc=1, device_id=peer, device_id_type=MESH)

    for k in range(3):
        loads[k].wait()

    def narrow(i):
        w[zl, y, rows32(i)] = w32[rows32(i)].astype(BF16)

    chunks(ALL, narrow)
    pl.semaphore_wait(barrier, len(peers))

    sends = []

    def remote(src, dst, send_sem, recv_sem, peer):
        return pltpu.make_async_remote_copy(
            src_ref=src, dst_ref=dst, send_sem=send_sem, recv_sem=recv_sem,
            device_id=peer, device_id_type=MESH,
        )

    class Gather:
        def __init__(self, base, lo, n, first_z):
            self.base, self.lo, self.n, self.first_z = base, lo, n, first_z

        def at(self, ia, ib, rows):
            if self.first_z:
                return w.at[zi(ia), yi(ib), rows]
            return w.at[zi(ib), yi(ia), rows]

        def blk(self, ia, ib):
            return self.at(ia, ib, pl.ds(self.lo, self.n))

        def half(self, ia, ib, h):
            return self.at(ia, ib, pl.ds(self.lo + h * (self.n // 2), self.n // 2))

        def peer_a(self, s):
            return near(0, s) if self.first_z else near(s, 0)

        def peer_b(self, s):
            return near(s, 0) if self.first_z else near(0, s)

        def send(self, k, ref, peer):
            k += self.base
            c = remote(ref, ref, ag_send.at[k], ag_recv.at[k], peer)
            c.start()
            sends.append(c)

        def got(self, k, ref):
            k += self.base
            remote(ref, ref, ag_send.at[k], ag_recv.at[k], near(1, 0)).wait_recv()

        def to_b(self, k, ia):
            self.send(k, self.blk(ia, 0), self.peer_b(1))
            self.send(k + 1, self.blk(ia, 0), self.peer_b(-1))

        def step(self, name):
            if name == "ag0":
                self.send(0, self.blk(0, 0), self.peer_a(1))
                self.send(1, self.blk(0, 0), self.peer_a(-1))
                self.to_b(2, 0)
            elif name == "a0":
                self.got(0, self.blk(-1, 0))
                self.send(4, self.half(-1, 0, 0), self.peer_a(1))
                self.to_b(6, -1)
            elif name == "a1":
                self.got(1, self.blk(1, 0))
                self.send(5, self.half(1, 0, 1), self.peer_a(-1))
                self.to_b(8, 1)
            elif name == "far":
                self.got(4, self.half(2, 0, 0))
                self.got(5, self.half(2, 0, 1))
                self.to_b(10, 2)
            elif name == "last":
                for n in range(4):
                    ia = (0, -1, 1, 2)[n]
                    self.got(12 + 2 * n, self.half(ia, 2, 0))
                    self.got(13 + 2 * n, self.half(ia, 2, 1))
            elif name[0] == "b":
                n = int(name[1])
                ia, k = (0, -1, 1, 2)[n], (2, 6, 8, 10)[n]
                if name[2] == "+":
                    self.got(k, self.blk(ia, -1))
                    self.send(12 + 2 * n, self.half(ia, -1, 0), self.peer_b(1))
                else:
                    self.got(k + 1, self.blk(ia, 1))
                    self.send(13 + 2 * n, self.half(ia, 1, 1), self.peer_b(-1))
            else:
                return False
            return True

    class Reduce:
        def __init__(self, base, lo, n, first_z):
            self.base, self.lo, self.n, self.first_z = base, lo, n, first_z
            h = n // 2
            self.rows = pl.ds(lo, n)
            self.half = (pl.ds(lo, h), pl.ds(lo + h, h))
            self.small = pl.ds(lo // 2, h)

        def part(self, ia, h):
            if self.first_z:
                return grad.at[zi(ia), pl.ds(2 * h, 2), self.rows]
            return grad.at[pl.ds(2 * h, 2), yi(ia), self.rows]

        def ib(self, k):
            return yi(k) if self.first_z else zi(k)

        def peer_a(self, s):
            return near(0, s) if self.first_z else near(s, 0)

        def peer_b(self, s):
            return near(s, 0) if self.first_z else near(0, s)

        def send(self, k, src, dst, peer):
            k += self.base
            c = remote(src, dst, rs_send.at[k], rs_recv.at[k], peer)
            c.start()
            sends.append(c)

        def got(self, k, ref):
            k += self.base
            remote(ref, ref, rs_send.at[k], rs_recv.at[k], near(1, 0)).wait_recv()

        def far(self, s, h):
            return r1.at[h, pl.ds(0, 2), self.rows]

        def near_part(self, s, h):
            return r2.at[s, pl.ds(2 * h, 2), self.rows]

        def add_part(self, ia, h):
            for j in range(2):
                def body(i, j=j):
                    rows = rows32(self.lo + i)
                    at = (zi(ia), 2 * h + j, rows) if self.first_z else (2 * h + j, yi(ia), rows)
                    total = grad[at].astype(F32) + r1[h, j, rows].astype(F32)
                    grad[at] = total.astype(BF16)

                chunks(self.n, body)

        def sum_own(self, k):
            ib = self.ib(k)

            def body(i):
                rows = rows32(self.lo + i)
                at = (zi(0), ib, rows) if self.first_z else (ib, yi(0), rows)
                total = grad[at].astype(F32) + r2[0, ib, rows].astype(F32)
                total = total + r2[1, ib, rows].astype(F32)
                own[ib, rows] = total.astype(BF16)

            chunks(self.n, body)

        def add_half(self, k, h):
            ib = self.ib(k)

            def body(i):
                rows = rows32(self.lo + h * (self.n // 2) + i)
                total = own[ib, rows].astype(F32) + b1[h, rows32(self.lo // 2 + i)].astype(F32)
                own[ib, rows] = total.astype(BF16)

            chunks(self.n // 2, body)

        def step(self, name):
            if name == "rs0":
                self.send(0, self.part(2, 0), self.far(0, 0), self.peer_a(1))
                self.send(1, self.part(2, 1), self.far(1, 1), self.peer_a(-1))
                self.send(2, self.part(1, 1), self.near_part(0, 1), self.peer_a(1))
                self.send(3, self.part(-1, 0), self.near_part(1, 0), self.peer_a(-1))
            elif name == "p0":
                self.got(0, self.far(0, 0))
                self.add_part(1, 0)
                self.send(4, self.part(1, 0), self.near_part(0, 0), self.peer_a(1))
            elif name == "p1":
                self.got(1, self.far(1, 1))
                self.add_part(-1, 1)
                self.send(5, self.part(-1, 1), self.near_part(1, 1), self.peer_a(-1))
            elif name == "own":
                self.got(2, self.near_part(0, 1))
                self.got(3, self.near_part(1, 0))
                self.got(4, self.near_part(0, 0))
                self.got(5, self.near_part(1, 1))
                lo, hi = self.half
                self.sum_own(2)
                self.send(6, own.at[self.ib(2), lo], b1.at[0, self.small], self.peer_b(1))
                self.send(7, own.at[self.ib(2), hi], b1.at[1, self.small], self.peer_b(-1))
                self.sum_own(1)
                self.send(8, own.at[self.ib(1), hi], b2.at[0, hi], self.peer_b(1))
                self.sum_own(-1)
                self.send(9, own.at[self.ib(-1), lo], b2.at[1, lo], self.peer_b(-1))
                self.sum_own(0)
            elif name == "q0":
                lo = self.half[0]
                self.got(6, b1.at[0, self.small])
                self.add_half(1, 0)
                self.send(10, own.at[self.ib(1), lo], b2.at[0, lo], self.peer_b(1))
            elif name == "q1":
                hi = self.half[1]
                self.got(7, b1.at[1, self.small])
                self.add_half(-1, 1)
                self.send(11, own.at[self.ib(-1), hi], b2.at[1, hi], self.peer_b(-1))
            elif name == "fin":
                lo, hi = self.half
                self.got(8, b2.at[0, hi])
                self.got(9, b2.at[1, lo])
                self.got(10, b2.at[0, lo])
                self.got(11, b2.at[1, hi])
                ib = self.ib(0)

                def body(i):
                    rows = rows32(self.lo + i)
                    total = own[ib, rows].astype(F32) + b2[0, rows].astype(F32)
                    total = total + b2[1, rows].astype(F32)
                    final[rows] = total.astype(BF16)

                chunks(self.n, body)
                self.send(12, final.at[lo], q1.at[0, self.small], near(0, 2))
                self.send(13, final.at[hi], q1.at[1, self.small], near(0, -2))
            elif name == "y0":
                self.got(12, q1.at[0, self.small])
                self.send(14, q1.at[0, self.small], q2.at[self.half[0]], near(0, 2))
            elif name == "y1":
                self.got(13, q1.at[1, self.small])
                self.send(15, q1.at[1, self.small], q2.at[self.half[1]], near(0, -2))
            elif name == "arr":
                self.got(14, q2.at[self.half[0]])
                self.got(15, q2.at[self.half[1]])
                which = self.lo // FFL
                out_ref = (od_ref, og_ref, ou_ref)[which]

                def out(i):
                    rows = rows32(self.lo + i)
                    total = final[rows].astype(F32) + q2[rows].astype(F32)
                    to = rows32(self.lo - which * FFL + i)
                    if which == 0:
                        total = total * scales[2, to]
                    out_ref[to, :] = total

                chunks(self.n, out)
            else:
                return False
            return True

    def elementwise():
        for k, ref in enumerate((gs_ref, us_ref, ds_ref)):
            scales[k] = jnp.broadcast_to(ref[...], (LANES, FFL)).T
        loads[3].wait()
        loads[4].wait()

        def body(i):
            rows = rows32(i)
            g = gate[rows, :].astype(F32)
            u = up[rows, :].astype(F32)
            sig = jax.nn.sigmoid(g)
            act = g * sig
            hidden[rows, :] = (act * u).astype(BF16)
            down = scales[2, rows]
            gs = jnp.concatenate([scales[0, rows] * down] * 4, axis=1)
            us = jnp.concatenate([scales[1, rows] * down] * 4, axis=1)
            fg[rows, :] = u * sig * (1.0 + g * (1.0 - sig)) * gs
            fu[rows, :] = act * us

        chunks(FFL, body)

    def down_grads():
        loads[5].wait()

        @pl.loop(0, 8)
        def _(k):
            zz, yy = lax.div(k, 2), lax.rem(k, 2) * 2
            cols = pl.ds(pl.multiple_of(k * 256, 256), 256)
            out = jnp.dot(hidden[...], cot[:, cols], preferred_element_type=F32).astype(BF16)
            grad[zz, yy, pl.ds(0, FFL)] = out[:, :LANES]
            grad[zz, yy + 1, pl.ds(0, FFL)] = out[:, LANES:]

    def cotangents():
        @pl.loop(0, 2)
        def _(m):
            cols = pl.ds(pl.multiple_of(m * 256, 256), 256)
            whole = jnp.concatenate(
                [w[i // 4, i % 4, pl.ds(0, FFL)] for i in range(16)], axis=1
            )
            hc = lax.dot_general(
                whole, cot[cols, :], (((1,), (1,)), ((), ())), preferred_element_type=F32
            )
            bc[pl.ds(0, FFL), cols] = (hc * fg[:, cols]).astype(BF16)
            bc[pl.ds(FFL, FFL), cols] = (hc * fu[:, cols]).astype(BF16)

    def gate_up_grads():
        loads[6].wait()

        @pl.loop(0, 8)
        def _(k):
            zz, yy = lax.div(k, 2), lax.rem(k, 2) * 2
            cols = pl.ds(pl.multiple_of(k * 256, 256), 256)
            out = jnp.dot(bc[...], x[:, cols], preferred_element_type=F32).astype(BF16)
            grad[zz, yy, pl.ds(FFL, GU)] = out[:, :LANES]
            grad[zz, yy + 1, pl.ds(FFL, GU)] = out[:, LANES:]

    def partial_inputs():
        @pl.loop(0, NTP)
        def _(r):
            t = lax.rem(tp + r, NTP)
            zz, yy = lax.div(t, 2), lax.rem(t, 2) * 2
            rows = pl.ds(FFL, GU)
            both = jnp.concatenate([w[zz, yy, rows], w[zz, yy + 1, rows]], axis=1)
            part = lax.dot_general(
                bc[...], both, (((0,), (0,)), ((), ())), preferred_element_type=F32
            )
            tp_out[r] = part.astype(BF16)

        for r in range(1, NTP):
            c = remote(tp_out.at[r], tp_in.at[r], tp_send.at[r], tp_recv.at[r], tp_peer(r))
            c.start()
            sends.append(c)

    def input_grad():
        for r in range(1, NTP):
            remote(
                tp_in.at[r], tp_in.at[r], tp_send.at[r], tp_recv.at[r], tp_peer(r)
            ).wait_recv()

        def body(i):
            rows = rows32(i)
            total = tp_out[0, rows].astype(F32)
            for r in range(1, NTP):
                total = total + tp_in[r, rows].astype(F32)
            oi_ref[rows, :] = total.astype(BF16)

        chunks(TOK, body)

    gathers = {}
    reduces = {}
    for i, (name, lo, n, ag_z, rs_z) in enumerate(PIECES):
        gathers[name] = Gather(20 * i, lo, n, ag_z)
        reduces[name] = Reduce(16 * i, lo, n, rs_z)
    work = {
        "ew": elementwise, "down": down_grads, "hc": cotangents,
        "gu": gate_up_grads, "part": partial_inputs, "tp": input_grad,
    }
    for step in ORDER:
        name, *piece = step.split(" ")
        if not piece:
            work[name]()
        elif not gathers[piece[0]].step(name):
            assert reduces[piece[0]].step(name)

    for c in sends:
        c.wait_send()


def local(
    inputs, cotangent, gate_pre, up_pre, gate_weight, up_weight, down_weight,
    gate_scale, up_scale, down_scale,
):
    hbm = pl.BlockSpec(memory_space=pl.ANY)
    vmem = pl.BlockSpec(memory_space=pltpu.VMEM)
    sem = pltpu.SemaphoreType.DMA
    half = ALL // 2
    oi, og, ou, od = pl.pallas_call(
        kernel,
        out_shape=(
            jax.ShapeDtypeStruct((TOK, 256), BF16),
            jax.ShapeDtypeStruct((FFL, LANES), F32),
            jax.ShapeDtypeStruct((FFL, LANES), F32),
            jax.ShapeDtypeStruct((FFL, LANES), F32),
        ),
        in_specs=[hbm] * 7 + [vmem] * 3,
        out_specs=(vmem,) * 4,
        scratch_shapes=[
            pltpu.VMEM((TOK, D), BF16),
            pltpu.VMEM((TOK, D), BF16),
            pltpu.VMEM((FFL, TOK), BF16),
            pltpu.VMEM((FFL, TOK), BF16),
            pltpu.VMEM((ALL, LANES), F32),
            pltpu.VMEM((3, FFL, LANES), F32),
            pltpu.VMEM((FFL, TOK), BF16),
            pltpu.VMEM((FFL, TOK), F32),
            pltpu.VMEM((FFL, TOK), F32),
            pltpu.VMEM((GU, TOK), BF16),
            pltpu.VMEM((4, 4, ALL, LANES), BF16),
            pltpu.VMEM((4, 4, ALL, LANES), BF16),
            pltpu.VMEM((2, 2, ALL, LANES), BF16),
            pltpu.VMEM((2, 4, ALL, LANES), BF16),
            pltpu.VMEM((4, ALL, LANES), BF16),
            pltpu.VMEM((2, half, LANES), BF16),
            pltpu.VMEM((2, ALL, LANES), BF16),
            pltpu.VMEM((ALL, LANES), BF16),
            pltpu.VMEM((2, half, LANES), BF16),
            pltpu.VMEM((ALL, LANES), BF16),
            pltpu.VMEM((NTP, TOK, 256), BF16),
            pltpu.VMEM((NTP, TOK, 256), BF16),
            sem((7,)),
            sem((20 * len(PIECES),)),
            sem((20 * len(PIECES),)),
            sem((16 * len(PIECES),)),
            sem((16 * len(PIECES),)),
            sem((NTP,)),
            sem((NTP,)),
        ],
        compiler_params=pltpu.CompilerParams(
            collective_id=0, has_side_effects=True, vmem_limit_bytes=58 * 1024 * 1024
        ),
    )(
        inputs, cotangent, gate_pre.T, up_pre.T,
        down_weight.T, gate_weight.T, up_weight.T, gate_scale, up_scale, down_scale,
    )
    return oi, og.T, ou.T, od.T


def solution(mesh):
    rows = ("rep", "fs")
    in_specs = (
        P(rows, None), P(rows, None), P(rows, "tp"), P(rows, "tp"),
        P("fs", "tp"), P("fs", "tp"), P("fs", "tp"),
        P(None, "tp"), P(None, "tp"), P(None, "tp"),
    )
    out_specs = (P(rows, "tp"), P("fs", "tp"), P("fs", "tp"), P("fs", "tp"))
    return jax.shard_map(local, mesh=mesh, in_specs=in_specs, out_specs=out_specs, check_vma=False)
```

time: 316 us -> 131 us (0.41)
  waiting for transfers between devices: 208 us -> 0 us
  Pallas kernels: 0 us -> 124 us
  local copies, waits for them, and re-layouts: 35.2 us -> 5.94 us
  blocking collectives: 19.3 us -> 0 us
  matrix products: 17 us -> 0 us
  between operations: 14 us -> 0.65 us
  starting transfers between devices: 11.5 us -> 0 us
  other arithmetic: 10.1 us -> 0 us
    pallas_call x0 -> x1, Pallas kernels: none -> 124 us  [local(): pl.pallas_call(kernel, out_shape=(jax.ShapeDtypeStruct((TOK, 256), BF16),...]
    unnamed x5 -> x0, waiting for transfers between devices: 95 us -> none
    all_gather x3 -> x0, waiting for transfers between devices: 86.2 us -> none  [stacked_from(): parts = lax.all_gather(parts, axes[k])]
    all_to_all x2 -> x0, waiting for transfers between devices: 26.5 us -> none  [the longest x1 26.5 us: copy_for_each(): return lax.all_to_all(copies, axis, split_axis=0, concat_axis=0, tiled=True)]
    all_gather x1 -> x0, blocking collectives: 19.3 us -> none  [stacked_from(): parts = lax.all_gather(parts, axes[k])]
    dot_general x5 -> x0, matrix products: 17 us -> none  [the longest x1 4.99 us: local(): lax.dot_general(cotangent, hidden, dims, preferred_element_type=jnp.float32)]
    all_to_all x2 -> x0, starting transfers between devices: 11.4 us -> none  [the longest x1 7 us: copy_for_each(): return lax.all_to_all(copies, axis, split_axis=0, concat_axis=0, tiled=True)]
    transpose x2 -> x0, local copies, waits for them, and re-layouts: 9.04 us -> none  [stacked_from(): parts = parts.transpose(*back, *range(len(axes), parts.ndim))]
  transfers between devices with their start and end apart: 6 -> 0, of which waited for: 5 -> 0; matrix products, arithmetic and copies ran while one was open for 18% -> 0% of each run, Pallas kernels for 0% -> 0%
where the time goes in v2:
time: 131 us
  Pallas kernels  124 us (95%)
  local copies, waits for them, and re-layouts  5.94 us (5%)
    pallas_call x1, Pallas kernels, local(): pl.pallas_call(kernel, out_shape=(jax.ShapeDtypeStruct((TOK, 256), BF16),...  124 us
    unnamed x6, local copies, waits for them, and re-layouts  5.94 us

profile of v2, /device:TPU:32, one launch (start us, length us, event | category | flops | bytes accessed | tf_op | source)
XLA Modules:
  0.0 131.0 jit_solution(3918362151105346506)
XLA Ops:
  0.6 124.4 %shard_map.129 = (bf16[512,256]{1,0:T(8,128)(2,1)}, f32[704,128]{1,0:T(8,128)}, f32[704,128]{1,0:T(8,128)}, f32[704,128]{1,0:T(8,128)}) custom-call(bf16[512,2048]{1,0:T(8,128)(2,1)} %x_hbm.1, bf16[512,2048]{1,0:T(8,128)(2,1)} %cot_hbm.1, bf16[704,512]{1,0:T(8,128)(2,1)} %bitcast.8, bf16[704,512]{1,0:T(8,128)(2,1)} %bitcast.9, f32[704,128]{1,0:T(8,128)} %bitcast.13, ...), custom_call_target="tpu_custom_call" | custom-call | tf_op jit(solution)/shard_map/pallas_call | solution.py:446
  125.0 0.0 copy-start
  125.0 1.7 %copy.18 = bf16[512,256]{1,0:T(8,128)(2,1)} copy(bf16[512,256]{1,0:T(8,128)(2,1)} %get-tuple-element.16) | data formatting | bytes 524288
  126.8 1.7 %copy.19 = f32[128,704]{0,1:T(8,128)} copy(f32[128,704]{0,1:T(8,128)} %bitcast.12) | data formatting | bytes 720896
  128.5 1.7 %copy.20 = f32[128,704]{0,1:T(8,128)} copy(f32[128,704]{0,1:T(8,128)} %bitcast.11) | data formatting | bytes 720896
  130.2 0.0 copy-done
  130.2 0.7 copy.21
Async XLA Ops:
  125.0 5.2 %copy-start = (f32[704,128]{1,0:T(8,128)S(1)}, f32[704,128]{1,0:T(8,128)}, u32[]{:S(2)}) copy-start(f32[704,128]{1,0:T(8,128)} %get-tuple-element.11) | copy-start | bytes 1081348

commit v3 on v0

v3 whole, which is shorter than its diff:
```python
import jax
import jax.numpy as jnp
from jax import lax
from jax.experimental import pallas as pl
from jax.experimental.pallas import tpu as pltpu
from jax.sharding import PartitionSpec as P

MESH = pl.DeviceIdType.MESH
F32 = jnp.float32
BF16 = jnp.bfloat16
LANES = 128
TOK = 512
HT = TOK // 2
D = 2048
QD = D // 4
FFL = 704
GU = 2 * FFL
ALL = 3 * FFL
H = FFL // 2
Q = FFL // 4
SIDES = (0, -1, 1, 2)

ORDER = (
    "st 1", "st 0", "ys 0 0", "ys 1 0", "ys 1 1", "ys 1 2", "yr 0 0 -1", "ys 1 3", "sc",
    "ys 0 3", "ys 0 1", "st 2", "c0", "ys 2 3", "sgu", "ys 0 2", "ys 2 2", "yr 0 1 -1",
    "yr 1 3 1", "c1", "ys 2 0", "yr 2 3 -1", "sx", "ys 2 1", "ew", "yr 1 1 -1", "yr 2 2 1",
    "yr 2 0 1", "yr 0 3 -1", "c2", "yr 1 3 -1", "yr 0 2 1", "yr 1 2 1", "yr 0 1 1",
    "yr 0 2 -1", "yr 2 2 -1", "yr 0 3 1", "down", "x0", "yr 2 0 -1", "yr 0 0 1", "yr 1 0 1",
    "yt 0 -1", "yr 2 1 1", "yr 2 1 -1", "ps 0", "yr 2 3 1", "rs 0", "yt 2 1", "yr 1 2 -1",
    "yt 2 -1", "yf 0", "yt 0 1", "last 0", "x1", "hc", "x2", "r+ 0", "r- 0", "gu 2", "yf 2",
    "yr 1 1 1", "ps 2", "yr 1 0 -1", "rs 2", "own 0", "gu 1", "ps 1", "yf 1", "yt 1 1",
    "yt 1 -1", "r- 2", "r+ 2", "fin 0", "rs 1", "own 2", "last 1", "last 2", "y 0 1", "y 0 0",
    "part", "r+ 1", "r- 1", "fin 2", "own 1", "y 2 0", "p 0", "p 1", "y 2 1", "fin 1", "arr 0",
    "psum", "y 1 1", "arr 2", "y 1 0", "tp", "arr 1",
)

def kernel(
    x_hbm, cot_hbm, gate_hbm, up_hbm, wd_hbm, wg_hbm, wu_hbm, gs_ref, us_ref, ds_ref,
    oi_ref, og_ref, ou_ref, od_ref,
    x, cot, gate, up, w32, scales, down_col, hidden, fg, fu, bc,
    w, mine, grad, sib, r1, r2, own, zr, zs, final, q1, q2,
    tp_out, xr1, xr2, from_home, from_guest,
    local_sem, send_sem, recv_sem,
):
    rep = lax.axis_index("rep")
    fs = lax.axis_index("fs")
    tp = lax.axis_index("tp")
    y = lax.rem(fs, 4)
    zl = lax.div(fs, 4)
    z = rep * 4 + zl
    xx = lax.div(tp, 2)
    h = lax.rem(tp, 2)
    p = lax.rem(zl, 2)
    home = h == p
    guest = h != p

    def dev(dx, dy, dz, core):
        nx = lax.rem(xx + dx + 4, 4)
        ny = lax.rem(y + dy + 4, 4)
        nz = lax.rem(z + dz + 8, 8)
        return (lax.div(nz, 4), lax.rem(nz, 4) * 4 + ny, nx * 2 + core)

    def yi(k):
        return lax.rem(y + k + 4, 4)

    def zi(k):
        return lax.rem(zl + k + 4, 4)

    def chunks(n, size, fn):
        if n == size:
            fn(0, size)
            return

        @pl.loop(0, n // size)
        def _(i):
            fn(i * size, size)

    def span(start, size):
        return pl.ds(start if isinstance(start, int) else pl.multiple_of(start, 16), size)

    def half(i, k):
        return pl.ds(pl.multiple_of(i * FFL + k * H, 16), H)

    def quarter(i, k, q):
        return pl.ds(pl.multiple_of(i * FFL + k * H + q * Q, 16), Q)

    def small(i):
        return pl.ds(i * H, H)

    send_ids, recv_ids = {}, {}
    sends = []

    def remote(src, dst, s, r, peer):
        return pltpu.make_async_remote_copy(
            src_ref=src, dst_ref=dst, send_sem=send_sem.at[s], recv_sem=recv_sem.at[r],
            device_id=peer, device_id_type=MESH,
        )

    def rid(name, spread):
        key = name if spread is None else (*name, "by")
        if key not in recv_ids:
            recv_ids[key] = sum(recv_sizes)
            recv_sizes.append(1 if spread is None else 2)
        return recv_ids[key] if spread is None else recv_ids[key] + spread

    recv_sizes = []

    def send(name, src, dst, peer, tag="", by=None):
        s = send_ids.setdefault((*name, tag), len(send_ids))
        remote(src, dst, s, rid(name, by), peer).start()
        sends.append((None, lambda: (src, dst, peer), s))

    def send_if(cond, name, make, tag=""):
        s = send_ids.setdefault((*name, tag), len(send_ids))
        src, dst, peer = make()
        remote(src, dst, s, rid(name, None), peer).start()
        sends.append((cond, make, s))

    def got(name, dst, by=None):
        remote(dst, dst, 0, rid(name, by), dev(0, 1, 0, h)).wait_recv()

    loads = []
    for k, (src, dst) in enumerate(
        (
            (wd_hbm, w32.at[pl.ds(0, FFL)]),
            (wg_hbm, w32.at[pl.ds(FFL, FFL)]),
            (wu_hbm, w32.at[pl.ds(GU, FFL)]),
            (gate_hbm, gate),
            (up_hbm, up),
            (cot_hbm, cot),
            (x_hbm, x),
        )
    ):
        loads.append(pltpu.make_async_copy(src, dst, local_sem.at[k]))
    for k in range(3):
        loads[k].start()

    barrier = pltpu.get_barrier_semaphore()
    peers = [dev(0, 1, 0, h), dev(0, -1, 0, h), dev(1, 0, 0, h), dev(-1, 0, 0, h)]
    for core in range(2):
        peers += [dev(0, 0, k, core) for k in (1, -1, 2, -2)]
    peers.append(dev(0, 0, 0, 1 - h))
    for peer in peers:
        pl.semaphore_signal(barrier, inc=1, device_id=peer, device_id_type=MESH)

    @pl.when(home)
    def _():
        for k in range(3, 7):
            loads[k].start()

    for k in range(3):
        loads[k].wait()

    @pl.when(home)
    def _():
        def narrow(i, n):
            w[zl, y, span(i, n)] = w32[span(i, n)].astype(BF16)

        chunks(ALL, Q, narrow)

    @pl.when(guest)
    def _():
        def narrow(i, n):
            mine[span(i, n)] = w32[span(i, n)].astype(BF16)

        chunks(ALL, Q, narrow)

    pl.semaphore_wait(barrier, len(peers))

    def other(core):
        return dev(0, 0, 0, core)

    def start(i):
        whole = pl.ds(i * FFL, FFL)

        @pl.when(home)
        def _():
            send_if(
                True, (i, "own"),
                lambda: (w.at[zl, y, whole], w.at[zl, y, whole], other(1 - h)),
            )
            for k in range(2):
                for q, s in ((0, 2), (1, -2)):
                    def make(k=k, q=q, s=s):
                        ref = w.at[zl, y, quarter(i, k, q)]
                        return ref, ref, dev(0, 0, s, k)

                    send_if(True, (i, "zq", q), make, k)

        @pl.when(guest)
        def _():
            for k in range(2):
                for s in (1, -1):
                    def make(k=k, s=s):
                        rows = half(i, k)
                        return mine.at[rows], w.at[zl, y, rows], dev(0, 0, s, k)

                    send_if(False, (i, "z", s), make, k)

    def swap(src, dst, name, wide):
        @pl.when(guest)
        def _():
            for s, part in ((1, pl.ds(0, HT)), (-1, pl.ds(HT, HT))):
                def make(s=s, part=part):
                    at = (part, qcols(0)) if wide else (slice(None), part)
                    return src.at[at], dst.at[at], dev(0, 0, s, p)

                send_if(False, (name, s), make)

    def swapped(dst, name, wide):
        for s, part in ((1, pl.ds(0, HT)), (-1, pl.ds(HT, HT))):
            at = (part, qcols(0)) if wide else (slice(None), part)
            got((name, s), dst.at[at])

    def qcols(k):
        return pl.ds(pl.multiple_of(lax.rem(xx + k + 4, 4) * QD, QD), QD)

    def spread0(dst, name):
        @pl.when(guest)
        def _():
            swapped(dst, name, True)
            for s in (1, -1):
                def make(s=s):
                    ref = dst.at[:, qcols(0)]
                    return ref, ref, dev(s, 0, 0, h)

                send_if(False, (name, "x", s), make)

    def spread1(dst, name):
        @pl.when(guest)
        def _():
            for s, part in ((1, pl.ds(0, HT)), (-1, pl.ds(HT, HT))):
                got((name, "x", s), dst.at[:, qcols(-s)])

                def make(s=s, part=part):
                    ref = dst.at[part, qcols(-s)]
                    return ref, ref, dev(s, 0, 0, h)

                send_if(False, (name, "xf", s), make)

    def spread2(dst, name, load):
        @pl.when(guest)
        def _():
            for s, part in ((1, pl.ds(0, HT)), (-1, pl.ds(HT, HT))):
                got((name, "xf", s), dst.at[part, qcols(2)])

        @pl.when(home)
        def _():
            loads[load].wait()

    def ys(i, c):
        ref = w.at[zi(SIDES[c]), y, half(i, h)]
        if c == 0:
            @pl.when(guest)
            def _():
                whole = pl.ds(i * FFL, FFL)
                got((i, "own"), w.at[zl, y, whole])
        elif c < 3:
            got((i, "z", -SIDES[c]), ref)
        else:
            for q in range(2):
                got((i, "zq", q), w.at[zi(2), y, quarter(i, h, q)])
        for s in (1, -1):
            send((i, "y", c, s), ref, ref, dev(0, s, 0, h))
        if c:
            send((i, "s", c), ref, ref, other(1 - h))

    def yr(i, c, s):
        got((i, "y", c, s), w.at[zi(SIDES[c]), yi(-s), half(i, h)])
        q = 0 if s == 1 else 1
        ref = w.at[zi(SIDES[c]), yi(-s), quarter(i, h, q)]
        send((i, "f", c, s), ref, ref, dev(0, s, 0, h))

    def yt(i, s):
        ref = w.at[:, yi(-s), half(i, h)]
        send((i, "t", s), ref, ref, other(1 - h))

    def yf(i):
        for c in range(4):
            for s, q in ((1, 0), (-1, 1)):
                got((i, "f", c, s), w.at[zi(SIDES[c]), yi(2), quarter(i, h, q)])
        yt(i, 2)

    def last(i):
        for c in range(1, 4):
            got((i, "s", c), w.at[zi(SIDES[c]), y, half(i, 1 - h)])
        for s in (1, -1, 2):
            got((i, "t", s), w.at[:, yi(-s), half(i, 1 - h)])

    def elementwise():
        down_col[...] = jnp.broadcast_to(ds_ref[...], (LANES, FFL)).T

        @pl.when(home)
        def _():
            for k, ref in enumerate((gs_ref, us_ref, ds_ref)):
                scales[k] = jnp.broadcast_to(ref[...], (LANES, FFL)).T
            send_if(True, ("scales",), lambda: (scales, scales, other(1 - h)))
            loads[3].wait()
            loads[4].wait()

        @pl.when(guest)
        def _():
            got(("scales",), scales)
            swapped(gate, "gate", False)
            swapped(up, "up", False)

        def body(i, n):
            rows = span(i, n)
            g = gate[rows, :].astype(F32)
            u = up[rows, :].astype(F32)
            sig = jax.nn.sigmoid(g)
            act = g * sig
            hidden[rows, :] = (act * u).astype(BF16)
            down = scales[2, rows]
            gs = jnp.concatenate([scales[0, rows] * down] * 4, axis=1)
            us = jnp.concatenate([scales[1, rows] * down] * 4, axis=1)
            fg[rows, :] = u * sig * (1.0 + g * (1.0 - sig)) * gs
            fu[rows, :] = act * us

        chunks(FFL, 16, body)

    def down_grads():
        @pl.loop(0, 8)
        def _(k):
            zz, yy = lax.div(k, 2), lax.rem(k, 2) * 2
            cols = pl.ds(pl.multiple_of(k * 256, 256), 256)
            out = jnp.dot(hidden[...], cot[:, cols], preferred_element_type=F32).astype(BF16)
            grad[zz, yy, pl.ds(0, FFL)] = out[:, :LANES]
            grad[zz, yy + 1, pl.ds(0, FFL)] = out[:, LANES:]

    def cotangents():
        @pl.loop(0, 2)
        def _(m):
            cols = pl.ds(pl.multiple_of(m * 256, 256), 256)
            whole = jnp.concatenate(
                [w[i // 4, i % 4, pl.ds(0, FFL)] for i in range(16)], axis=1
            )
            hc = lax.dot_general(
                whole, cot[cols, :], (((1,), (1,)), ((), ())), preferred_element_type=F32
            )
            bc[pl.ds(0, FFL), cols] = (hc * fg[:, cols]).astype(BF16)
            bc[pl.ds(FFL, FFL), cols] = (hc * fu[:, cols]).astype(BF16)

    def gate_up_grads(i):
        @pl.loop(0, 8)
        def _(k):
            zz, yy = lax.div(k, 2), lax.rem(k, 2) * 2
            cols = pl.ds(pl.multiple_of(k * 256, 256), 256)
            units = pl.ds((i - 1) * FFL, FFL)
            out = jnp.dot(bc[units, :], x[:, cols], preferred_element_type=F32).astype(BF16)
            grad[zz, yy, pl.ds(i * FFL, FFL)] = out[:, :LANES]
            grad[zz, yy + 1, pl.ds(i * FFL, FFL)] = out[:, LANES:]

    def presum(i):
        for k in (2, 1, -1, 0):
            src = grad.at[:, yi(k), half(i, 1 - h)]
            send((i, "ps", k), src, sib.at[:, yi(k), small(i)], other(1 - h))

    def add(i, k, b, *more):
        def body(j, n):
            at = (b, yi(k), span(i * FFL + h * H + j, n))
            total = grad[at].astype(F32) + sib[b, yi(k), span(i * H + j, n)].astype(F32)
            for ref in more:
                total = total + ref[span(i * H + j, n)].astype(F32)
            grad[at] = total.astype(BF16)

        chunks(H, Q, body)

    def part(i, k, b):
        return grad.at[pl.ds(b, 2), yi(k), half(i, h)]

    def got_sib(i, k):
        got((i, "ps", k), sib.at[:, yi(k), small(i)])

    def rs_start(i):
        got_sib(i, 2)
        for b in range(2):
            add(i, 2, b)
        send((i, "r", 0), part(i, 2, 0), r1.at[0, :, small(i)], dev(0, 1, 0, h))
        for b in range(2, 4):
            add(i, 2, b)
        send((i, "r", 1), part(i, 2, 2), r1.at[1, :, small(i)], dev(0, -1, 0, h))
        got_sib(i, 1)
        for b in range(2, 4):
            add(i, 1, b)
        send((i, "r", 2), part(i, 1, 2), r2.at[0, pl.ds(2, 2), small(i)], dev(0, 1, 0, h))
        got_sib(i, -1)
        for b in range(2):
            add(i, -1, b)
        send((i, "r", 3), part(i, -1, 0), r2.at[1, pl.ds(0, 2), small(i)], dev(0, -1, 0, h))

    def rs_plus(i):
        got((i, "r", 0), r1.at[0, :, small(i)])
        for b in range(2):
            add(i, 1, b, r1.at[0, b])
        send((i, "r", 4), part(i, 1, 0), r2.at[0, pl.ds(0, 2), small(i)], dev(0, 1, 0, h))

    def rs_minus(i):
        got((i, "r", 1), r1.at[1, :, small(i)])
        for b in range(2, 4):
            add(i, -1, b, r1.at[1, b - 2])
        send((i, "r", 5), part(i, -1, 2), r2.at[1, pl.ds(2, 2), small(i)], dev(0, -1, 0, h))

    def sum_own(i, k):
        b = zi(k)

        def body(j, n):
            rows = span(i * H + j, n)
            total = grad[b, yi(0), span(i * FFL + h * H + j, n)].astype(F32)
            total = total + sib[b, yi(0), rows].astype(F32)
            total = total + r2[0, b, rows].astype(F32) + r2[1, b, rows].astype(F32)
            own[b, rows] = total.astype(BF16)

        chunks(H, Q, body)

    def rs_own(i):
        got_sib(i, 0)
        got((i, "r", 2), r2.at[0, pl.ds(2, 2), small(i)])
        got((i, "r", 3), r2.at[1, pl.ds(0, 2), small(i)])
        got((i, "r", 4), r2.at[0, pl.ds(0, 2), small(i)])
        got((i, "r", 5), r2.at[1, pl.ds(2, 2), small(i)])
        sum_own(i, 2)
        for q, s in ((0, 2), (1, -2)):
            src = own.at[zi(2), pl.ds(i * H + q * Q, Q)]
            send((i, "g", q), src, zr.at[q, quarter(i, h, q)], dev(0, 0, s, p), by=h)
        for q, s in ((0, 1), (1, -1)):
            sum_own(i, s)
            src = own.at[zi(s), small(i)]
            send((i, "n", q), src, zr.at[q, half(i, h)], dev(0, 0, s, p), by=h)
        sum_own(i, 0)

        @pl.when(guest)
        def _():
            send_if(
                False, (i, "zs"), lambda: (own.at[zl, small(i)], zs.at[small(i)], other(p))
            )

    def rs_fin(i):
        @pl.when(home)
        def _():
            for k in range(2):
                for q in range(2):
                    got((i, "g", q), zr.at[q, quarter(i, k, q)], by=k)
            got((i, "zs"), zs.at[small(i)])
            for q in range(2):
                def body(j, n, q=q):
                    low = span(i * H + q * Q + j, n)
                    rows = span(i * FFL + h * H + q * Q + j, n)
                    total = own[zl, low].astype(F32) + zr[q, rows].astype(F32)
                    final[rows] = total.astype(BF16)
                    rows = span(i * FFL + (1 - h) * H + q * Q + j, n)
                    total = zs[low].astype(F32) + zr[q, rows].astype(F32)
                    final[rows] = total.astype(BF16)

                chunks(Q, Q, body)

        @pl.when(guest)
        def _():
            for k in range(2):
                for q in range(2):
                    got((i, "n", q), zr.at[q, half(i, k)], by=k)

            def body(j, n):
                rows = span(i * FFL + j, n)
                total = zr[0, rows].astype(F32) + zr[1, rows].astype(F32)
                final[rows] = total.astype(BF16)

            chunks(FFL, Q, body)

        for q, s in ((0, 2), (1, -2)):
            send((i, "e", q), final.at[half(i, q)], q1.at[q, small(i)], dev(0, 0, s, h))

    def relay(i, q):
        got((i, "e", q), q1.at[q, small(i)])
        s = (2, -2)[q]
        send((i, "k", q), q1.at[q, small(i)], q2.at[half(i, q)], dev(0, 0, s, h))

    def arrive(i):
        for q in range(2):
            got((i, "k", q), q2.at[half(i, q)])
        out_ref = (od_ref, og_ref, ou_ref)[i]

        def body(j, n):
            rows = span(i * FFL + j, n)
            total = final[rows].astype(F32) + q2[rows].astype(F32)
            if i == 0:
                total = total * down_col[span(j, n)]
            out_ref[span(j, n), :] = total

        chunks(FFL, Q, body)

    def partial_inputs():
        @pl.loop(0, 8)
        def _(r):
            t = lax.rem(xx * 2 + r, 8)
            zz, yy = lax.div(t, 2), lax.rem(t, 2) * 2
            rows = pl.ds(FFL, GU)
            both = jnp.concatenate([w[zz, yy, rows], w[zz, yy + 1, rows]], axis=1)
            value = lax.dot_general(
                bc[...], both, (((0,), (0,)), ((), ())), preferred_element_type=F32
            )
            tp_out[lax.div(r, 2), lax.rem(r, 2)] = value.astype(BF16)

        for k, s in ((0, 1), (1, -1)):
            send(("p", k), tp_out.at[2, :, tokens[k]], xr1.at[k], dev(s, 0, 0, h))
        send(("p", 2), tp_out.at[1, :, tokens[1]], xr2.at[0, :, tokens[1]], dev(1, 0, 0, h))
        send(("p", 3), tp_out.at[3, :, tokens[0]], xr2.at[1, :, tokens[0]], dev(-1, 0, 0, h))

    tokens = (pl.ds(0, HT), pl.ds(HT, HT))

    def partial_on(k):
        s = (1, -1)[k]
        got(("p", k), xr1.at[k])
        for core in range(2):
            def body(j, n, core=core):
                at = (s % 4, core, span(k * HT + j, n))
                total = tp_out[at].astype(F32) + xr1[k, core, span(j, n)].astype(F32)
                tp_out[at] = total.astype(BF16)

            chunks(HT, 128, body)
        send(
            ("p", 4 + k), tp_out.at[s % 4, :, tokens[k]], xr2.at[k, :, tokens[k]],
            dev(s, 0, 0, h),
        )

    def partial_sum():
        got(("p", 2), xr2.at[0, :, tokens[1]])
        got(("p", 3), xr2.at[1, :, tokens[0]])
        got(("p", 4), xr2.at[0, :, tokens[0]])
        got(("p", 5), xr2.at[1, :, tokens[1]])
        for core in range(2):
            def body(j, n, core=core):
                rows = span(j, n)
                total = tp_out[0, core, rows].astype(F32) + xr2[0, core, rows].astype(F32)
                total = total + xr2[1, core, rows].astype(F32)
                tp_out[0, core, rows] = total.astype(BF16)

            chunks(TOK, 128, body)

        @pl.when(home)
        def _():
            send_if(
                True, ("h",), lambda: (tp_out.at[0, 1 - h], from_home, other(1 - h))
            )

            def keep(j, n):
                from_home[span(j, n)] = tp_out[0, h, span(j, n)]

            chunks(TOK, 128, keep)

        @pl.when(guest)
        def _():
            for core in range(2):
                for s, rows in ((-1, tokens[0]), (1, tokens[1])):
                    def make(core=core, s=s, rows=rows):
                        return tp_out.at[0, core, rows], from_guest.at[rows], dev(0, 0, s, core)

                    send_if(False, ("g", s), make, core)

    def input_grad():
        @pl.when(guest)
        def _():
            got(("h",), from_home)

        for s, rows in ((-1, tokens[0]), (1, tokens[1])):
            got(("g", s), from_guest.at[rows])

        def body(j, n):
            rows = span(j, n)
            total = from_home[rows].astype(F32) + from_guest[rows].astype(F32)
            oi_ref[rows, :] = total.astype(BF16)

        chunks(TOK, 128, body)

    work = {
        "st": start, "ys": ys, "yr": yr, "yt": yt, "yf": yf, "last": last,
        "ew": elementwise, "down": down_grads, "hc": cotangents, "gu": gate_up_grads,
        "part": partial_inputs, "p": partial_on, "psum": partial_sum, "tp": input_grad, "ps": presum, "rs": rs_start,
        "r+": rs_plus, "r-": rs_minus, "own": rs_own, "fin": rs_fin, "y": relay, "arr": arrive,
        "sgu": lambda: (swap(gate_hbm, gate, "gate", False), swap(up_hbm, up, "up", False)),
        "sc": lambda: swap(cot_hbm, cot, "cot", True),
        "sx": lambda: swap(x_hbm, x, "x", True),
        "c0": lambda: spread0(cot, "cot"), "c1": lambda: spread1(cot, "cot"),
        "c2": lambda: spread2(cot, "cot", 5),
        "x0": lambda: spread0(x, "x"), "x1": lambda: spread1(x, "x"),
        "x2": lambda: spread2(x, "x", 6),
    }
    for step in ORDER:
        name, *args = step.split(" ")
        work[name](*(int(a) for a in args))
    assert len(send_ids) <= SEMS and sum(recv_sizes) <= SEMS, (len(send_ids), sum(recv_sizes))

    for cond in (None, True, False):
        def drain(cond=cond):
            for c, make, s in sends:
                if c is cond:
                    src, dst, peer = make()
                    remote(src, dst, s, 0, peer).wait_send()

        if cond is None:
            drain()
        else:
            pl.when(home if cond else guest)(drain)


SEMS = 256


def local(
    inputs, cotangent, gate_pre, up_pre, gate_weight, up_weight, down_weight,
    gate_scale, up_scale, down_scale,
):
    hbm = pl.BlockSpec(memory_space=pl.ANY)
    vmem = pl.BlockSpec(memory_space=pltpu.VMEM)
    sem = pltpu.SemaphoreType.DMA
    half = ALL // 2
    oi, og, ou, od = pl.pallas_call(
        kernel,
        out_shape=(
            jax.ShapeDtypeStruct((TOK, 256), BF16),
            jax.ShapeDtypeStruct((FFL, LANES), F32),
            jax.ShapeDtypeStruct((FFL, LANES), F32),
            jax.ShapeDtypeStruct((FFL, LANES), F32),
        ),
        in_specs=[hbm] * 7 + [vmem] * 3,
        out_specs=(vmem,) * 4,
        scratch_shapes=[
            pltpu.VMEM((TOK, D), BF16),
            pltpu.VMEM((TOK, D), BF16),
            pltpu.VMEM((FFL, TOK), BF16),
            pltpu.VMEM((FFL, TOK), BF16),
            pltpu.VMEM((ALL, LANES), F32),
            pltpu.VMEM((3, FFL, LANES), F32),
            pltpu.VMEM((FFL, LANES), F32),
            pltpu.VMEM((FFL, TOK), BF16),
            pltpu.VMEM((FFL, TOK), F32),
            pltpu.VMEM((FFL, TOK), F32),
            pltpu.VMEM((GU, TOK), BF16),
            pltpu.VMEM((4, 4, ALL, LANES), BF16),
            pltpu.VMEM((ALL, LANES), BF16),
            pltpu.VMEM((4, 4, ALL, LANES), BF16),
            pltpu.VMEM((4, 4, half, LANES), BF16),
            pltpu.VMEM((2, 2, half, LANES), BF16),
            pltpu.VMEM((2, 4, half, LANES), BF16),
            pltpu.VMEM((4, half, LANES), BF16),
            pltpu.VMEM((2, ALL, LANES), BF16),
            pltpu.VMEM((half, LANES), BF16),
            pltpu.VMEM((ALL, LANES), BF16),
            pltpu.VMEM((2, half, LANES), BF16),
            pltpu.VMEM((ALL, LANES), BF16),
            pltpu.VMEM((4, 2, TOK, 256), BF16),
            pltpu.VMEM((2, 2, HT, 256), BF16),
            pltpu.VMEM((2, 2, TOK, 256), BF16),
            pltpu.VMEM((TOK, 256), BF16),
            pltpu.VMEM((TOK, 256), BF16),
            sem((7,)),
            sem((SEMS,)),
            sem((SEMS,)),
        ],
        compiler_params=pltpu.CompilerParams(
            collective_id=0, has_side_effects=True, vmem_limit_bytes=58 * 1024 * 1024
        ),
    )(
        inputs, cotangent, gate_pre.T, up_pre.T,
        down_weight.T, gate_weight.T, up_weight.T, gate_scale, up_scale, down_scale,
    )
    return oi, og.T, ou.T, od.T


def solution(mesh):
    rows = ("rep", "fs")
    in_specs = (
        P(rows, None), P(rows, None), P(rows, "tp"), P(rows, "tp"),
        P("fs", "tp"), P("fs", "tp"), P("fs", "tp"),
        P(None, "tp"), P(None, "tp"), P(None, "tp"),
    )
    out_specs = (P(rows, "tp"), P("fs", "tp"), P("fs", "tp"), P("fs", "tp"))
    return jax.shard_map(local, mesh=mesh, in_specs=in_specs, out_specs=out_specs, check_vma=False)
```

time: 316 us -> 120 us (0.38)
  waiting for transfers between devices: 208 us -> 0 us
  Pallas kernels: 0 us -> 113 us
  local copies, waits for them, and re-layouts: 35.2 us -> 5.94 us
  blocking collectives: 19.3 us -> 0 us
  matrix products: 17 us -> 0 us
  between operations: 14 us -> 0.65 us
  starting transfers between devices: 11.5 us -> 0 us
  other arithmetic: 10.1 us -> 0 us
    pallas_call x0 -> x1, Pallas kernels: none -> 113 us  [local(): pl.pallas_call(kernel, out_shape=(jax.ShapeDtypeStruct((TOK, 256), BF16),...]
    unnamed x5 -> x0, waiting for transfers between devices: 95 us -> none
    all_gather x3 -> x0, waiting for transfers between devices: 86.2 us -> none  [stacked_from(): parts = lax.all_gather(parts, axes[k])]
    all_to_all x2 -> x0, waiting for transfers between devices: 26.5 us -> none  [the longest x1 26.5 us: copy_for_each(): return lax.all_to_all(copies, axis, split_axis=0, concat_axis=0, tiled=True)]
    all_gather x1 -> x0, blocking collectives: 19.3 us -> none  [stacked_from(): parts = lax.all_gather(parts, axes[k])]
    dot_general x5 -> x0, matrix products: 17 us -> none  [the longest x1 4.99 us: local(): lax.dot_general(cotangent, hidden, dims, preferred_element_type=jnp.float32)]
    all_to_all x2 -> x0, starting transfers between devices: 11.4 us -> none  [the longest x1 7 us: copy_for_each(): return lax.all_to_all(copies, axis, split_axis=0, concat_axis=0, tiled=True)]
    transpose x2 -> x0, local copies, waits for them, and re-layouts: 9.04 us -> none  [stacked_from(): parts = parts.transpose(*back, *range(len(axes), parts.ndim))]
  transfers between devices with their start and end apart: 6 -> 0, of which waited for: 5 -> 0; matrix products, arithmetic and copies ran while one was open for 18% -> 0% of each run, Pallas kernels for 0% -> 0%
where the time goes in v3:
time: 120 us; the launch traced here: 119 us
  Pallas kernels  113 us (94%)
  local copies, waits for them, and re-layouts  5.94 us (5%)
    pallas_call x1, Pallas kernels, local(): pl.pallas_call(kernel, out_shape=(jax.ShapeDtypeStruct((TOK, 256), BF16),...  113 us
    unnamed x6, local copies, waits for them, and re-layouts  5.94 us

profile of v3, /device:TPU:32, one launch (start us, length us, event | category | flops | bytes accessed | tf_op | source)
XLA Modules:
  0.0 119.5 jit_solution(16259219833093944548)
XLA Ops:
  0.6 112.9 %shard_map.129 = (bf16[512,256]{1,0:T(8,128)(2,1)}, f32[704,128]{1,0:T(8,128)}, f32[704,128]{1,0:T(8,128)}, f32[704,128]{1,0:T(8,128)}) custom-call(bf16[512,2048]{1,0:T(8,128)(2,1)} %x_hbm.1, bf16[512,2048]{1,0:T(8,128)(2,1)} %cot_hbm.1, bf16[704,512]{1,0:T(8,128)(2,1)} %bitcast.8, bf16[704,512]{1,0:T(8,128)(2,1)} %bitcast.9, f32[704,128]{1,0:T(8,128)} %bitcast.13, ...), custom_call_target="tpu_custom_call" | custom-call | tf_op jit(solution)/shard_map/pallas_call | solution.py:617
  113.5 0.0 copy-start
  113.5 1.7 %copy.18 = bf16[512,256]{1,0:T(8,128)(2,1)} copy(bf16[512,256]{1,0:T(8,128)(2,1)} %get-tuple-element.16) | data formatting | bytes 524288
  115.2 1.7 %copy.19 = f32[128,704]{0,1:T(8,128)} copy(f32[128,704]{0,1:T(8,128)} %bitcast.12) | data formatting | bytes 720896
  117.0 1.7 %copy.20 = f32[128,704]{0,1:T(8,128)} copy(f32[128,704]{0,1:T(8,128)} %bitcast.11) | data formatting | bytes 720896
  118.7 0.0 copy-done
  118.7 0.7 copy.21
Async XLA Ops:
  113.5 5.2 %copy-start = (f32[704,128]{1,0:T(8,128)S(1)}, f32[704,128]{1,0:T(8,128)}, u32[]{:S(2)}) copy-start(f32[704,128]{1,0:T(8,128)} %get-tuple-element.11) | copy-start | bytes 1081348

commit v4 on v3

--- a/solution.py
+++ b/solution.py
@@ -16,27 +16,26 @@
 FFL = 704
 GU = 2 * FFL
 ALL = 3 * FFL
-H = FFL // 2
-Q = FFL // 4
 SIDES = (0, -1, 1, 2)
 
+PIECES = ((0, 704), (704, 704), (1408, 704))
 ORDER = (
-    "st 1", "st 0", "ys 0 0", "ys 1 0", "ys 1 1", "ys 1 2", "yr 0 0 -1", "ys 1 3", "sc",
-    "ys 0 3", "ys 0 1", "st 2", "c0", "ys 2 3", "sgu", "ys 0 2", "ys 2 2", "yr 0 1 -1",
-    "yr 1 3 1", "c1", "ys 2 0", "yr 2 3 -1", "sx", "ys 2 1", "ew", "yr 1 1 -1", "yr 2 2 1",
-    "yr 2 0 1", "yr 0 3 -1", "c2", "yr 1 3 -1", "yr 0 2 1", "yr 1 2 1", "yr 0 1 1",
-    "yr 0 2 -1", "yr 2 2 -1", "yr 0 3 1", "down", "x0", "yr 2 0 -1", "yr 0 0 1", "yr 1 0 1",
-    "yt 0 -1", "yr 2 1 1", "yr 2 1 -1", "ps 0", "yr 2 3 1", "rs 0", "yt 2 1", "yr 1 2 -1",
-    "yt 2 -1", "yf 0", "yt 0 1", "last 0", "x1", "hc", "x2", "r+ 0", "r- 0", "gu 2", "yf 2",
-    "yr 1 1 1", "ps 2", "yr 1 0 -1", "rs 2", "own 0", "gu 1", "ps 1", "yf 1", "yt 1 1",
-    "yt 1 -1", "r- 2", "r+ 2", "fin 0", "rs 1", "own 2", "last 1", "last 2", "y 0 1", "y 0 0",
-    "part", "r+ 1", "r- 1", "fin 2", "own 1", "y 2 0", "p 0", "p 1", "y 2 1", "fin 1", "arr 0",
-    "psum", "y 1 1", "arr 2", "y 1 0", "tp", "arr 1",
+    "st 1", "sc", "st 0", "ys 1 0", "st 2", "ys 2 0", "yr 1 0 1", "ys 0 0", "yr 1 0 -1",
+    "ys 1 1", "ys 1 2", "sgu", "ys 1 3", "c0", "ys 0 3", "ys 0 2", "ys 2 3", "yr 0 3 -1",
+    "ys 0 1", "c1", "yr 1 2 1", "yr 0 2 1", "sx", "yr 0 3 1", "yr 1 2 -1", "ys 2 2",
+    "yr 1 3 1", "yr 2 0 -1", "ew", "yr 0 1 1", "yr 0 0 -1", "c2", "yr 0 2 -1", "yr 1 3 -1",
+    "yr 1 1 -1", "yr 2 0 1", "yr 0 0 1", "ys 2 1", "yt 0 1", "down", "ps 0", "x0", "yr 0 1 -1",
+    "yr 2 3 1", "rs 0", "yf 0", "yt 0 -1", "yr 2 2 1", "last 0", "yr 2 2 -1", "x1", "hc",
+    "r+ 0", "yr 2 1 1", "r- 0", "yr 1 1 1", "yt 1 -1", "yt 2 1", "x2", "yr 2 3 -1",
+    "yr 2 1 -1", "yt 1 1", "gu 1", "ps 1", "rs 1", "own 0", "gu 2", "ps 2", "r- 1", "r+ 1",
+    "yf 2", "yf 1", "yt 2 -1", "fin 0", "rs 2", "last 2", "own 1", "y 0 1", "y 0 0", "last 1",
+    "part", "r- 2", "r+ 2", "fin 1", "own 2", "y 1 1", "p 1", "y 1 0", "p 0", "fin 2", "psum",
+    "arr 1", "y 2 0", "y 2 1", "arr 0", "tp", "arr 2",
 )
 
 def kernel(
     x_hbm, cot_hbm, gate_hbm, up_hbm, wd_hbm, wg_hbm, wu_hbm, gs_ref, us_ref, ds_ref,
-    oi_ref, og_ref, ou_ref, od_ref,
+    oi_ref, out_ref,
     x, cot, gate, up, w32, scales, down_col, hidden, fg, fu, bc,
     w, mine, grad, sib, r1, r2, own, zr, zs, final, q1, q2,
     tp_out, xr1, xr2, from_home, from_guest,
@@ -78,14 +77,21 @@
     def span(start, size):
         return pl.ds(start if isinstance(start, int) else pl.multiple_of(start, 16), size)
 
+    def whole(i):
+        lo, n = PIECES[i]
+        return pl.ds(lo, n)
+
     def half(i, k):
-        return pl.ds(pl.multiple_of(i * FFL + k * H, 16), H)
+        lo, n = PIECES[i]
+        return pl.ds(pl.multiple_of(lo + k * (n // 2), 16), n // 2)
 
     def quarter(i, k, q):
-        return pl.ds(pl.multiple_of(i * FFL + k * H + q * Q, 16), Q)
+        lo, n = PIECES[i]
+        return pl.ds(pl.multiple_of(lo + k * (n // 2) + q * (n // 4), 16), n // 4)
 
     def small(i):
-        return pl.ds(i * H, H)
+        lo, n = PIECES[i]
+        return pl.ds(lo // 2, n // 2)
 
     send_ids, recv_ids = {}, {}
     sends = []
@@ -156,14 +162,14 @@
         def narrow(i, n):
             w[zl, y, span(i, n)] = w32[span(i, n)].astype(BF16)
 
-        chunks(ALL, Q, narrow)
+        chunks(ALL, 176, narrow)
 
     @pl.when(guest)
     def _():
         def narrow(i, n):
             mine[span(i, n)] = w32[span(i, n)].astype(BF16)
 
-        chunks(ALL, Q, narrow)
+        chunks(ALL, 176, narrow)
 
     pl.semaphore_wait(barrier, len(peers))
 
@@ -171,13 +177,11 @@
         return dev(0, 0, 0, core)
 
     def start(i):
-        whole = pl.ds(i * FFL, FFL)
-
         @pl.when(home)
         def _():
             send_if(
                 True, (i, "own"),
-                lambda: (w.at[zl, y, whole], w.at[zl, y, whole], other(1 - h)),
+                lambda: (w.at[zl, y, whole(i)], w.at[zl, y, whole(i)], other(1 - h)),
             )
             for k in range(2):
                 for q, s in ((0, 2), (1, -2)):
@@ -253,8 +257,7 @@
         if c == 0:
             @pl.when(guest)
             def _():
-                whole = pl.ds(i * FFL, FFL)
-                got((i, "own"), w.at[zl, y, whole])
+                got((i, "own"), w.at[zl, y, whole(i)])
         elif c < 3:
             got((i, "z", -SIDES[c]), ref)
         else:
@@ -332,11 +335,11 @@
         @pl.loop(0, 2)
         def _(m):
             cols = pl.ds(pl.multiple_of(m * 256, 256), 256)
-            whole = jnp.concatenate(
+            rows = jnp.concatenate(
                 [w[i // 4, i % 4, pl.ds(0, FFL)] for i in range(16)], axis=1
             )
             hc = lax.dot_general(
-                whole, cot[cols, :], (((1,), (1,)), ((), ())), preferred_element_type=F32
+                rows, cot[cols, :], (((1,), (1,)), ((), ())), preferred_element_type=F32
             )
             bc[pl.ds(0, FFL), cols] = (hc * fg[:, cols]).astype(BF16)
             bc[pl.ds(FFL, FFL), cols] = (hc * fu[:, cols]).astype(BF16)
@@ -346,10 +349,10 @@
         def _(k):
             zz, yy = lax.div(k, 2), lax.rem(k, 2) * 2
             cols = pl.ds(pl.multiple_of(k * 256, 256), 256)
-            units = pl.ds((i - 1) * FFL, FFL)
-            out = jnp.dot(bc[units, :], x[:, cols], preferred_element_type=F32).astype(BF16)
-            grad[zz, yy, pl.ds(i * FFL, FFL)] = out[:, :LANES]
-            grad[zz, yy + 1, pl.ds(i * FFL, FFL)] = out[:, LANES:]
+            lo, n = PIECES[i]
+            out = jnp.dot(bc[pl.ds(lo - FFL, n), :], x[:, cols], preferred_element_type=F32).astype(BF16)
+            grad[zz, yy, whole(i)] = out[:, :LANES]
+            grad[zz, yy + 1, whole(i)] = out[:, LANES:]
 
     def presum(i):
         for k in (2, 1, -1, 0):
@@ -357,14 +360,17 @@
             send((i, "ps", k), src, sib.at[:, yi(k), small(i)], other(1 - h))
 
     def add(i, k, b, *more):
+        lo, size = PIECES[i]
+
         def body(j, n):
-            at = (b, yi(k), span(i * FFL + h * H + j, n))
-            total = grad[at].astype(F32) + sib[b, yi(k), span(i * H + j, n)].astype(F32)
+            at = (b, yi(k), span(lo + h * (size // 2) + j, n))
+            low = span(lo // 2 + j, n)
+            total = grad[at].astype(F32) + sib[b, yi(k), low].astype(F32)
             for ref in more:
-                total = total + ref[span(i * H + j, n)].astype(F32)
+                total = total + ref[low].astype(F32)
             grad[at] = total.astype(BF16)
 
-        chunks(H, Q, body)
+        chunks(size // 2, size // 4, body)
 
     def part(i, k, b):
         return grad.at[pl.ds(b, 2), yi(k), half(i, h)]
@@ -403,15 +409,16 @@
 
     def sum_own(i, k):
         b = zi(k)
+        lo, size = PIECES[i]
 
         def body(j, n):
-            rows = span(i * H + j, n)
-            total = grad[b, yi(0), span(i * FFL + h * H + j, n)].astype(F32)
+            rows = span(lo // 2 + j, n)
+            total = grad[b, yi(0), span(lo + h * (size // 2) + j, n)].astype(F32)
             total = total + sib[b, yi(0), rows].astype(F32)
             total = total + r2[0, b, rows].astype(F32) + r2[1, b, rows].astype(F32)
             own[b, rows] = total.astype(BF16)
 
-        chunks(H, Q, body)
+        chunks(size // 2, size // 4, body)
 
     def rs_own(i):
         got_sib(i, 0)
@@ -419,9 +426,10 @@
         got((i, "r", 3), r2.at[1, pl.ds(0, 2), small(i)])
         got((i, "r", 4), r2.at[0, pl.ds(0, 2), small(i)])
         got((i, "r", 5), r2.at[1, pl.ds(2, 2), small(i)])
+        lo, n = PIECES[i]
         sum_own(i, 2)
         for q, s in ((0, 2), (1, -2)):
-            src = own.at[zi(2), pl.ds(i * H + q * Q, Q)]
+            src = own.at[zi(2), pl.ds(lo // 2 + q * (n // 4), n // 4)]
             send((i, "g", q), src, zr.at[q, quarter(i, h, q)], dev(0, 0, s, p), by=h)
         for q, s in ((0, 1), (1, -1)):
             sum_own(i, s)
@@ -436,6 +444,9 @@
             )
 
     def rs_fin(i):
+        lo, size = PIECES[i]
+        hn, qn = size // 2, size // 4
+
         @pl.when(home)
         def _():
             for k in range(2):
@@ -444,15 +455,15 @@
             got((i, "zs"), zs.at[small(i)])
             for q in range(2):
                 def body(j, n, q=q):
-                    low = span(i * H + q * Q + j, n)
-                    rows = span(i * FFL + h * H + q * Q + j, n)
+                    low = span(lo // 2 + q * qn + j, n)
+                    rows = span(lo + h * hn + q * qn + j, n)
                     total = own[zl, low].astype(F32) + zr[q, rows].astype(F32)
                     final[rows] = total.astype(BF16)
-                    rows = span(i * FFL + (1 - h) * H + q * Q + j, n)
+                    rows = span(lo + (1 - h) * hn + q * qn + j, n)
                     total = zs[low].astype(F32) + zr[q, rows].astype(F32)
                     final[rows] = total.astype(BF16)
 
-                chunks(Q, Q, body)
+                chunks(qn, qn, body)
 
         @pl.when(guest)
         def _():
@@ -461,11 +472,11 @@
                     got((i, "n", q), zr.at[q, half(i, k)], by=k)
 
             def body(j, n):
-                rows = span(i * FFL + j, n)
+                rows = span(lo + j, n)
                 total = zr[0, rows].astype(F32) + zr[1, rows].astype(F32)
                 final[rows] = total.astype(BF16)
 
-            chunks(FFL, Q, body)
+            chunks(size, qn, body)
 
         for q, s in ((0, 2), (1, -2)):
             send((i, "e", q), final.at[half(i, q)], q1.at[q, small(i)], dev(0, 0, s, h))
@@ -478,16 +489,16 @@
     def arrive(i):
         for q in range(2):
             got((i, "k", q), q2.at[half(i, q)])
-        out_ref = (od_ref, og_ref, ou_ref)[i]
+        lo, size = PIECES[i]
 
         def body(j, n):
-            rows = span(i * FFL + j, n)
+            rows = span(lo + j, n)
             total = final[rows].astype(F32) + q2[rows].astype(F32)
-            if i == 0:
-                total = total * down_col[span(j, n)]
-            out_ref[span(j, n), :] = total
-
-        chunks(FFL, Q, body)
+            if lo < FFL:
+                total = total * down_col[rows]
+            out_ref[rows, :] = total
+
+        chunks(size, size // 4, body)
 
     def partial_inputs():
         @pl.loop(0, 8)
@@ -606,6 +617,23 @@
 SEMS = 256
 
 
+def hand_out(oi_in, all_in, oi_out, og_out, ou_out, od_out, oi, grads, in_sem, out_sem):
+    pieces = [(oi_in, oi, oi_out)]
+    for k, ref in enumerate((od_out, og_out, ou_out)):
+        rows = pl.ds(k * FFL, FFL)
+        pieces.append((all_in.at[rows], grads.at[rows], ref))
+    copies = []
+    for k, (src, mid, dst) in enumerate(pieces):
+        first = pltpu.make_async_copy(src, mid, in_sem.at[k])
+        first.start()
+        copies.append((first, pltpu.make_async_copy(mid, dst, out_sem.at[k])))
+    for first, second in copies:
+        first.wait()
+        second.start()
+    for _, second in copies:
+        second.wait()
+
+
 def local(
     inputs, cotangent, gate_pre, up_pre, gate_weight, up_weight, down_weight,
     gate_scale, up_scale, down_scale,
@@ -614,16 +642,14 @@
     vmem = pl.BlockSpec(memory_space=pltpu.VMEM)
     sem = pltpu.SemaphoreType.DMA
     half = ALL // 2
-    oi, og, ou, od = pl.pallas_call(
+    oi, out = pl.pallas_call(
         kernel,
         out_shape=(
             jax.ShapeDtypeStruct((TOK, 256), BF16),
-            jax.ShapeDtypeStruct((FFL, LANES), F32),
-            jax.ShapeDtypeStruct((FFL, LANES), F32),
-            jax.ShapeDtypeStruct((FFL, LANES), F32),
+            jax.ShapeDtypeStruct((ALL, LANES), F32),
         ),
         in_specs=[hbm] * 7 + [vmem] * 3,
-        out_specs=(vmem,) * 4,
+        out_specs=(vmem,) * 2,
         scratch_shapes=[
             pltpu.VMEM((TOK, D), BF16),
             pltpu.VMEM((TOK, D), BF16),
@@ -664,6 +690,21 @@
         inputs, cotangent, gate_pre.T, up_pre.T,
         down_weight.T, gate_weight.T, up_weight.T, gate_scale, up_scale, down_scale,
     )
+    oi, og, ou, od = pl.pallas_call(
+        hand_out,
+        out_shape=(
+            jax.ShapeDtypeStruct((TOK, 256), BF16),
+            jax.ShapeDtypeStruct((FFL, LANES), F32),
+            jax.ShapeDtypeStruct((FFL, LANES), F32),
+            jax.ShapeDtypeStruct((FFL, LANES), F32),
+        ),
+        in_specs=[hbm] * 2,
+        out_specs=(hbm,) * 4,
+        scratch_shapes=[
+            pltpu.VMEM((TOK, 256), BF16), pltpu.VMEM((ALL, LANES), F32), sem((4,)), sem((4,)),
+        ],
+        compiler_params=pltpu.CompilerParams(vmem_limit_bytes=60 * 1024 * 1024),
+    )(oi, out)
     return oi, og.T, ou.T, od.T
 
 

time: 120 us -> 115 us (0.958)
  local copies, waits for them, and re-layouts: 5.94 us -> 0 us
    unnamed x6 -> x0, local copies, waits for them, and re-layouts: 5.94 us -> none
    pallas_call x0 -> x1, Pallas kernels: none -> 2.11 us  [local(): pl.pallas_call(hand_out, out_shape=(jax.ShapeDtypeStruct((TOK, 256), BF16...]
    pallas_call x1, Pallas kernels: 113 us -> 111 us  [local(): pl.pallas_call(kernel, out_shape=(jax.ShapeDtypeStruct((TOK, 256), BF16),...]
where the time goes in v4:
time: 115 us; the launch traced here: 114 us
  Pallas kernels  113 us (98%)
    pallas_call x1, Pallas kernels, local(): pl.pallas_call(kernel, out_shape=(jax.ShapeDtypeStruct((TOK, 256), BF16),...  111 us

profile of v4, /device:TPU:32, one launch (start us, length us, event | category | flops | bytes accessed | tf_op | source)
XLA Modules:
  0.0 114.1 jit_solution(12186381839328845172)
XLA Ops:
  0.6 111.3 %shard_map.129 = (bf16[512,256]{1,0:T(8,128)(2,1)}, f32[2112,128]{1,0:T(8,128)}) custom-call(bf16[512,2048]{1,0:T(8,128)(2,1)} %x_hbm.1, bf16[512,2048]{1,0:T(8,128)(2,1)} %cot_hbm.1, bf16[704,512]{1,0:T(8,128)(2,1)} %bitcast.8, bf16[704,512]{1,0:T(8,128)(2,1)} %bitcast.9, f32[704,128]{1,0:T(8,128)} %bitcast.10, f32[704,128]{1,0:T(8,128)} %bitcast.11, ...), custom_call_target="tpu_custom_call" | custom-call | tf_op jit(solution)/shard_map/pallas_call | solution.py:645
  112.0 2.1 %shard_map.130 = (bf16[512,256]{1,0:T(8,128)(2,1)}, f32[704,128]{1,0:T(8,128)}, f32[704,128]{1,0:T(8,128)}, f32[704,128]{1,0:T(8,128)}) custom-call(bf16[512,256]{1,0:T(8,128)(2,1)} %get-tuple-element.10.oi_in, f32[2112,128]{1,0:T(8,128)} %get-tuple-element.11.all_in), custom_call_target="tpu_custom_call" | custom-call | tf_op jit(solution)/shard_map/pallas_call | solution.py:693

commit v5 on v4

--- a/solution.py
+++ b/solution.py
@@ -20,17 +20,17 @@
 
 PIECES = ((0, 704), (704, 704), (1408, 704))
 ORDER = (
-    "st 1", "sc", "st 0", "ys 1 0", "st 2", "ys 2 0", "yr 1 0 1", "ys 0 0", "yr 1 0 -1",
-    "ys 1 1", "ys 1 2", "sgu", "ys 1 3", "c0", "ys 0 3", "ys 0 2", "ys 2 3", "yr 0 3 -1",
-    "ys 0 1", "c1", "yr 1 2 1", "yr 0 2 1", "sx", "yr 0 3 1", "yr 1 2 -1", "ys 2 2",
-    "yr 1 3 1", "yr 2 0 -1", "ew", "yr 0 1 1", "yr 0 0 -1", "c2", "yr 0 2 -1", "yr 1 3 -1",
-    "yr 1 1 -1", "yr 2 0 1", "yr 0 0 1", "ys 2 1", "yt 0 1", "down", "ps 0", "x0", "yr 0 1 -1",
-    "yr 2 3 1", "rs 0", "yf 0", "yt 0 -1", "yr 2 2 1", "last 0", "yr 2 2 -1", "x1", "hc",
-    "r+ 0", "yr 2 1 1", "r- 0", "yr 1 1 1", "yt 1 -1", "yt 2 1", "x2", "yr 2 3 -1",
-    "yr 2 1 -1", "yt 1 1", "gu 1", "ps 1", "rs 1", "own 0", "gu 2", "ps 2", "r- 1", "r+ 1",
-    "yf 2", "yf 1", "yt 2 -1", "fin 0", "rs 2", "last 2", "own 1", "y 0 1", "y 0 0", "last 1",
-    "part", "r- 2", "r+ 2", "fin 1", "own 2", "y 1 1", "p 1", "y 1 0", "p 0", "fin 2", "psum",
-    "arr 1", "y 2 0", "y 2 1", "arr 0", "tp", "arr 2",
+    "st 2", "sc", "st 0", "ys 0 0", "ys 2 0", "st 1", "ys 1 0", "ys 2 2", "ys 2 1", "ys 0 3",
+    "c0", "ys 2 3", "sgu", "sx", "yr 0 0 -1", "ys 1 3", "ys 0 1", "ys 0 2", "ys 1 1", "ys 1 2",
+    "c1", "yr 0 1 -1", "yr 0 3 1", "yr 0 2 1", "ew", "yr 2 2 1", "x0", "yr 0 3 -1",
+    "yr 2 3 -1", "yr 2 2 -1", "yr 0 2 -1", "yr 2 0 -1", "yr 1 0 -1", "yr 2 1 1", "c2",
+    "yr 0 0 1", "yr 0 1 1", "yt 0 -1", "yr 1 2 1", "yr 1 3 -1", "yr 1 1 -1", "yr 1 3 1",
+    "yr 1 1 1", "yr 1 2 -1", "yr 1 0 1", "yt 0 1", "down", "yr 2 0 1", "yr 2 1 -1", "ps 0",
+    "yf 0", "yt 1 1", "rs 0", "yt 2 -1", "x1", "yr 2 3 1", "last 0", "yf 1", "hc", "x2",
+    "r+ 0", "yt 2 1", "r- 0", "gu 1", "yf 2", "ps 1", "rs 1", "own 0", "gu 2", "yt 1 -1",
+    "last 2", "r- 1", "ps 2", "r+ 1", "fin 0", "rs 2", "own 1", "last 1", "part", "y 0 1",
+    "y 0 0", "fin 1", "r- 2", "r+ 2", "own 2", "y 1 1", "p 1", "y 1 0", "p 0", "fin 2", "psum",
+    "y 2 1", "y 2 0", "tp", "arr 1", "arr 0", "arr 2",
 )
 
 def kernel(
@@ -614,7 +614,7 @@
             pl.when(home if cond else guest)(drain)
 
 
-SEMS = 256
+SEMS = 288
 
 
 def hand_out(oi_in, all_in, oi_out, og_out, ou_out, od_out, oi, grads, in_sem, out_sem):

time: 115 us -> 113 us (0.983)
    pallas_call x1, Pallas kernels: 111 us -> 110 us  [local(): pl.pallas_call(kernel, out_shape=(jax.ShapeDtypeStruct((TOK, 256), BF16),...]
where the time goes in v5:
time: 113 us
  Pallas kernels  112 us (99%)
    pallas_call x1, Pallas kernels, local(): pl.pallas_call(kernel, out_shape=(jax.ShapeDtypeStruct((TOK, 256), BF16),...  110 us

profile of v5, /device:TPU:32, one launch (start us, length us, event | category | flops | bytes accessed | tf_op | source)
XLA Modules:
  0.0 112.7 jit_solution(511283579706904296)
XLA Ops:
  0.6 110.0 %shard_map.129 = (bf16[512,256]{1,0:T(8,128)(2,1)}, f32[2112,128]{1,0:T(8,128)}) custom-call(bf16[512,2048]{1,0:T(8,128)(2,1)} %x_hbm.1, bf16[512,2048]{1,0:T(8,128)(2,1)} %cot_hbm.1, bf16[704,512]{1,0:T(8,128)(2,1)} %bitcast.8, bf16[704,512]{1,0:T(8,128)(2,1)} %bitcast.9, f32[704,128]{1,0:T(8,128)} %bitcast.10, f32[704,128]{1,0:T(8,128)} %bitcast.11, ...), custom_call_target="tpu_custom_call" | custom-call | tf_op jit(solution)/shard_map/pallas_call | solution.py:645
  110.6 2.1 %shard_map.130 = (bf16[512,256]{1,0:T(8,128)(2,1)}, f32[704,128]{1,0:T(8,128)}, f32[704,128]{1,0:T(8,128)}, f32[704,128]{1,0:T(8,128)}) custom-call(bf16[512,256]{1,0:T(8,128)(2,1)} %get-tuple-element.10.oi_in, f32[2112,128]{1,0:T(8,128)} %get-tuple-element.11.all_in), custom_call_target="tpu_custom_call" | custom-call | tf_op jit(solution)/shard_map/pallas_call | solution.py:693

commit v6 on v5

--- a/solution.py
+++ b/solution.py
@@ -35,11 +35,11 @@
 
 def kernel(
     x_hbm, cot_hbm, gate_hbm, up_hbm, wd_hbm, wg_hbm, wu_hbm, gs_ref, us_ref, ds_ref,
-    oi_ref, out_ref,
+    oi_hbm, out_hbm,
     x, cot, gate, up, w32, scales, down_col, hidden, fg, fu, bc,
     w, mine, grad, sib, r1, r2, own, zr, zs, final, q1, q2,
     tp_out, xr1, xr2, from_home, from_guest,
-    local_sem, send_sem, recv_sem,
+    oi_ref, out_ref, local_sem, send_sem, recv_sem,
 ):
     rep = lax.axis_index("rep")
     fs = lax.axis_index("fs")
@@ -499,6 +499,13 @@
             out_ref[rows, :] = total
 
         chunks(size, size // 4, body)
+        leave(out_ref.at[whole(i)], out_hbm.at[whole(i)], 7 + i)
+
+    leaving = []
+
+    def leave(src, dst, k):
+        leaving.append(pltpu.make_async_copy(src, dst, local_sem.at[k]))
+        leaving[-1].start()
 
     def partial_inputs():
         @pl.loop(0, 8)
@@ -582,6 +589,7 @@
             oi_ref[rows, :] = total.astype(BF16)
 
         chunks(TOK, 128, body)
+        leave(oi_ref, oi_hbm, 10)
 
     work = {
         "st": start, "ys": ys, "yr": yr, "yt": yt, "yf": yf, "last": last,
@@ -601,6 +609,9 @@
         work[name](*(int(a) for a in args))
     assert len(send_ids) <= SEMS and sum(recv_sizes) <= SEMS, (len(send_ids), sum(recv_sizes))
 
+    for c in leaving:
+        c.wait()
+
     for cond in (None, True, False):
         def drain(cond=cond):
             for c, make, s in sends:
@@ -649,7 +660,7 @@
             jax.ShapeDtypeStruct((ALL, LANES), F32),
         ),
         in_specs=[hbm] * 7 + [vmem] * 3,
-        out_specs=(vmem,) * 2,
+        out_specs=(hbm,) * 2,
         scratch_shapes=[
             pltpu.VMEM((TOK, D), BF16),
             pltpu.VMEM((TOK, D), BF16),
@@ -679,7 +690,9 @@
             pltpu.VMEM((2, 2, TOK, 256), BF16),
             pltpu.VMEM((TOK, 256), BF16),
             pltpu.VMEM((TOK, 256), BF16),
-            sem((7,)),
+            pltpu.VMEM((TOK, 256), BF16),
+            pltpu.VMEM((ALL, LANES), F32),
+            sem((11,)),
             sem((SEMS,)),
             sem((SEMS,)),
         ],

time: 113 us -> 113 us (level)
  no operation moved by 1% of the time
where the time goes in v6:
time: 113 us; the launch traced here: 112 us
  Pallas kernels  112 us (99%)
    pallas_call x1, Pallas kernels, local(): pl.pallas_call(kernel, out_shape=(jax.ShapeDtypeStruct((TOK, 256), BF16),...  110 us

profile of v6, /device:TPU:32, one launch (start us, length us, event | category | flops | bytes accessed | tf_op | source)
XLA Modules:
  0.0 112.4 jit_solution(986168316042462513)
XLA Ops:
  0.6 109.6 %shard_map.129 = (bf16[512,256]{1,0:T(8,128)(2,1)}, f32[2112,128]{1,0:T(8,128)}) custom-call(bf16[512,2048]{1,0:T(8,128)(2,1)} %x_hbm.1, bf16[512,2048]{1,0:T(8,128)(2,1)} %cot_hbm.1, bf16[704,512]{1,0:T(8,128)(2,1)} %bitcast.8, bf16[704,512]{1,0:T(8,128)(2,1)} %bitcast.9, f32[704,128]{1,0:T(8,128)} %bitcast.10, f32[704,128]{1,0:T(8,128)} %bitcast.11, ...), custom_call_target="tpu_custom_call" | custom-call | tf_op jit(solution)/shard_map/pallas_call | solution.py:656
  110.3 2.1 %shard_map.130 = (bf16[512,256]{1,0:T(8,128)(2,1)}, f32[704,128]{1,0:T(8,128)}, f32[704,128]{1,0:T(8,128)}, f32[704,128]{1,0:T(8,128)}) custom-call(bf16[512,256]{1,0:T(8,128)(2,1)} %get-tuple-element.10.oi_in, f32[2112,128]{1,0:T(8,128)} %get-tuple-element.11.all_in), custom_call_target="tpu_custom_call" | custom-call | tf_op jit(solution)/shard_map/pallas_call | solution.py:706
